TPU v7x, 32 devices: a whole 2x2x4 slice. The times are simulated.
32 devices in a mesh: ep: 8 (over z, core), tp: 4 (over y, x).
Axes of the slice: x: 2, y: 2, z: 4, core: 2. Of those that a mesh axis runs over, the one named last changes fastest.
Arguments:
- tokens: bfloat16 [128, 2048], P('ep'), may hold values from -6 to 6
- attn_gain: float32 [2048], replicated, may hold values from 0.1 to 1.9
- query_weight: bfloat16 [2048, 2048], P('ep', 'tp'), may hold values from -0.125 to 0.125
- key_weight: bfloat16 [2048, 2048], P('ep', 'tp'), may hold values from -0.125 to 0.125
- value_weight: bfloat16 [2048, 2048], P('ep', 'tp'), may hold values from -0.125 to 0.125
- forget_weight: bfloat16 [2048, 16], P(None, 'tp'), may hold values from -0.125 to 0.125
- forget_bias: float32 [16], P('tp'), may hold values from -1 to 2
- cache_keys: bfloat16 [128, 16, 384, 128], P('ep', 'tp'), may hold values from -240 to 240
- cache_values: bfloat16 [128, 16, 384, 128], P('ep', 'tp'), may hold values from -6 to 6
- cache_gates: float32 [128, 16, 384], P('ep', 'tp'), may hold values from -768 to 0, as said below
- lengths: int32 [128], P('ep'), may hold values from 1 to 384
- output_weight: bfloat16 [2048, 2048], P('tp', 'ep'), may hold values from -0.125 to 0.125
- ffn_gain: float32 [2048], replicated, may hold values from 0.1 to 1.9
- dense_gate_proj: bfloat16 [2048, 2048], P('ep', 'tp'), may hold values from -0.125 to 0.125
- dense_up_proj: bfloat16 [2048, 2048], P('ep', 'tp'), may hold values from -0.125 to 0.125
- dense_down_proj: bfloat16 [2048, 2048], P('tp', 'ep'), may hold values from -0.125 to 0.125
- dense_mix: bfloat16 [2048], replicated, may hold values from -0.125 to 0.125
- expert_ids: int32 [128, 2], P('ep'), may hold values from 0 to 7, as said below
- group_prob: float32 [128], P('ep'), may hold values from 0.25 to 1
- pair_prob: float32 [128, 2], P('ep'), may hold values from 0.05 to 1
- expert_gate: bfloat16 [8, 2048, 2048], P('ep', None, 'tp'), may hold values from -0.125 to 0.125
- expert_up: bfloat16 [8, 2048, 2048], P('ep', None, 'tp'), may hold values from -0.125 to 0.125
- expert_down: bfloat16 [8, 2048, 2048], P('ep', 'tp'), may hold values from -0.125 to 0.125
Outputs:
- mixed_out: bfloat16 [128, 2048], P('ep')
Inputs may be any that keep to these rules, and one draw needn't show every extreme that they name: `expert_ids`: each row names two different experts of one group, the groups being 4 runs of consecutive ids. In each aligned block of 16 rows (the rows of one index of ep) no expert is named more than 8 times, and some expert exactly 8 times. `cache_gates`: along positions the values never rise.
All inputs are finite; a program needn't handle non-finite values.
Results may differ from a plain program's by a relative error of at most 0.014.
Values may be sent and summed in bfloat16 or wider, within the bound.
A program may use at most 64 MiB of HBM per device.

v0:
```python
import math

import jax
import jax.numpy as jnp
from jax import lax
from jax.sharding import PartitionSpec as P

EPSILON = 1e-06


def rms_scale(values, norm_gain):
    widened = values.astype(jnp.float32)
    return (
        widened
        * lax.rsqrt(jnp.mean(widened * widened, axis=-1, keepdims=True) + EPSILON)
        * norm_gain
    )


def attend(queries, keys_new, values_new, key_cache, value_cache, gate_cache, lengths, log_forget):
    cache_span = key_cache.shape[2]
    score_scale = 1.0 / math.sqrt(key_cache.shape[3])
    positions = jnp.arange(cache_span, dtype=jnp.int32)
    live_mask = positions[None, :] < lengths[:, None]
    last_mask = positions[None, :] == lengths[:, None] - 1
    last_gate = jnp.sum(jnp.where(last_mask[:, None, :], gate_cache, 0.0), axis=-1)
    gate_now = last_gate + log_forget
    scores = (
        jnp.einsum("shd,shpd->shp", queries, key_cache, preferred_element_type=jnp.float32)
        * score_scale
    )
    scores = scores + gate_now[:, :, None] - gate_cache
    scores = jnp.where(live_mask[:, None, :], scores, -jnp.inf)
    own_score = (
        jnp.sum(queries.astype(jnp.float32) * keys_new.astype(jnp.float32), axis=-1) * score_scale
    )
    row_top = jnp.maximum(jnp.max(scores, axis=-1), own_score)
    raised = jnp.exp(scores - row_top[:, :, None])
    own_raised = jnp.exp(own_score - row_top)
    totals = jnp.sum(raised, axis=-1) + own_raised
    weights_low = (raised / totals[:, :, None]).astype(jnp.bfloat16)
    own_prob = (own_raised / totals).astype(jnp.bfloat16)
    attended = jnp.einsum(
        "shp,shpd->shd", weights_low, value_cache, preferred_element_type=jnp.float32
    )
    attended = attended + own_prob.astype(jnp.float32)[:, :, None] * values_new.astype(jnp.float32)
    return attended.astype(jnp.bfloat16)


def row_term(spread, joined):
    return jnp.dot(spread, joined, preferred_element_type=jnp.float32)


def right_product(left_rows, weight_piece):
    return jnp.dot(left_rows, weight_piece, preferred_element_type=jnp.float32)


def shards(
    tokens,
    attn_gain,
    query_weight,
    key_weight,
    value_weight,
    forget_weight,
    forget_bias,
    cache_keys,
    cache_values,
    cache_gates,
    lengths,
    output_weight,
    ffn_gain,
    dense_gate_proj,
    dense_up_proj,
    dense_down_proj,
    dense_mix,
    expert_ids,
    group_prob,
    pair_prob,
    expert_gate,
    expert_up,
    expert_down,
):
    seq_count = tokens.shape[0]
    head_count = cache_keys.shape[1]
    head_size = cache_keys.shape[3]
    proj_width = query_weight.shape[1]
    normed = rms_scale(tokens, attn_gain).astype(jnp.bfloat16)
    spread = lax.all_to_all(normed, "ep", split_axis=1, concat_axis=0, tiled=True)
    joined = jnp.concatenate([query_weight, key_weight, value_weight], axis=1)
    summed = lax.psum_scatter(row_term(spread, joined), "ep", scatter_dimension=0, tiled=True)
    projected = (
        summed[:, :proj_width],
        summed[:, proj_width : 2 * proj_width],
        summed[:, 2 * proj_width :],
    )
    queries = projected[0].astype(jnp.bfloat16).reshape(seq_count, head_count, head_size)
    keys_new = projected[1].astype(jnp.bfloat16).reshape(seq_count, head_count, head_size)
    values_new = projected[2].astype(jnp.bfloat16).reshape(seq_count, head_count, head_size)
    log_forget = jax.nn.log_sigmoid(
        jnp.dot(normed, forget_weight, preferred_element_type=jnp.float32) + forget_bias
    )
    attended = attend(
        queries, keys_new, values_new, cache_keys, cache_values, cache_gates, lengths, log_forget
    )
    attended = attended.reshape(seq_count, head_count * head_size)
    head_terms = right_product(attended, lax.all_gather(output_weight, "ep", axis=1, tiled=True))
    mixed_heads = lax.psum(head_terms, "tp")
    residual = (tokens.astype(jnp.float32) + mixed_heads).astype(jnp.bfloat16)
    ffn_in = rms_scale(residual, ffn_gain).astype(jnp.bfloat16)
    dense_width = dense_gate_proj.shape[1]
    ffn_spread = lax.all_to_all(ffn_in, "ep", split_axis=1, concat_axis=0, tiled=True)
    dense_joined = jnp.concatenate([dense_gate_proj, dense_up_proj], axis=1)
    dense_summed = lax.psum_scatter(
        row_term(ffn_spread, dense_joined).astype(jnp.bfloat16),
        "ep",
        scatter_dimension=0,
        tiled=True,
    ).astype(jnp.float32)
    dense_parts = (dense_summed[:, :dense_width], dense_summed[:, dense_width:])
    dense_hidden = (jax.nn.silu(dense_parts[0]) * dense_parts[1]).astype(jnp.bfloat16)
    dense_terms = right_product(
        dense_hidden, lax.all_gather(dense_down_proj, "ep", axis=1, tiled=True)
    )
    dense_total = lax.psum(dense_terms.astype(jnp.bfloat16), "tp").astype(jnp.float32)
    mix = jax.nn.sigmoid(jnp.dot(ffn_in, dense_mix, preferred_element_type=jnp.float32))
    expert_count = lax.axis_size("ep") * expert_gate.shape[0]
    capacity = 4 * seq_count // expert_count
    slot_total = expert_count * capacity
    picks = expert_ids.reshape(-1)
    expert_grid = jnp.arange(expert_count, dtype=jnp.int32)
    pick_onehot = (picks[:, None] == expert_grid[None, :]).astype(jnp.int32)
    earlier = jnp.cumsum(pick_onehot, axis=0) - pick_onehot
    slot_rank = jnp.sum(earlier * pick_onehot, axis=1)
    destination = (picks * capacity + slot_rank).reshape(seq_count, 2)
    slot_grid = jnp.arange(slot_total, dtype=jnp.int32)
    select_first = (destination[:, 0:1] == slot_grid[None, :]).astype(jnp.bfloat16)
    select_second = (destination[:, 1:2] == slot_grid[None, :]).astype(jnp.bfloat16)
    selector = select_first + select_second
    outbound = jnp.einsum("sk,sd->kd", selector, ffn_in, preferred_element_type=jnp.float32)
    outbound = outbound.astype(jnp.bfloat16).reshape(expert_count, capacity, ffn_in.shape[1])
    arrived = lax.all_to_all(outbound, "ep", split_axis=0, concat_axis=0, tiled=True)
    sources, slots_now, feature = arrived.shape
    row_data = arrived.reshape(sources * slots_now, feature)
    gate_part = jnp.dot(row_data, expert_gate[0], preferred_element_type=jnp.float32)
    up_part = jnp.dot(row_data, expert_up[0], preferred_element_type=jnp.float32)
    expert_hidden = (jax.nn.silu(gate_part) * up_part).astype(jnp.bfloat16)
    partial_out = jnp.dot(expert_hidden, expert_down[0], preferred_element_type=jnp.float32)
    expert_result = lax.psum(partial_out.astype(jnp.bfloat16), "tp").astype(jnp.float32)
    returned = lax.all_to_all(
        expert_result.reshape(sources, slots_now, feature).astype(jnp.bfloat16),
        "ep",
        split_axis=0,
        concat_axis=0,
        tiled=True,
    ).astype(jnp.float32)
    returned = returned.reshape(slot_total, ffn_in.shape[1])
    routes = group_prob[:, None] * pair_prob / jnp.sum(pair_prob, axis=1, keepdims=True)
    first_back = returned[destination[:, 0]]
    second_back = returned[destination[:, 1]]
    side_total = (
        routes[:, 0:1] * first_back + routes[:, 1:2] * second_back + mix[:, None] * dense_total
    )
    result = residual.astype(jnp.float32) + side_total
    return result.astype(jnp.bfloat16)


def solution(mesh):
    return jax.shard_map(
        shards,
        mesh=mesh,
        in_specs=(
            P("ep", None),
            P(),
            P("ep", "tp"),
            P("ep", "tp"),
            P("ep", "tp"),
            P(None, "tp"),
            P("tp"),
            P("ep", "tp", None, None),
            P("ep", "tp", None, None),
            P("ep", "tp", None),
            P("ep"),
            P("tp", "ep"),
            P(),
            P("ep", "tp"),
            P("ep", "tp"),
            P("tp", "ep"),
            P(),
            P("ep", None),
            P("ep"),
            P("ep", None),
            P("ep", None, "tp"),
            P("ep", None, "tp"),
            P("ep", "tp", None),
        ),
        out_specs=P("ep", None),
        check_vma=False,
    )
```

profile of v0, /device:TPU:0, one launch (start us, length us, event | category | flops | bytes accessed | tf_op | source)
XLA Modules:
  0.0 268.5 jit_solution(17298867801017753038)
XLA Ops:
  6.6 1.1 fusion.32
  7.7 0.9 fusion.34
  8.7 12.1 %all_to_all.48 = bf16[16,8,256]{2,0,1:T(8,128)(2,1)S(1)} all-to-all(bf16[16,8,256]{2,0,1:T(8,128)(2,1)S(1)} %bitcast.96), channel_id=1, replica_groups=mesh['ep'=8,'tp'=4] {'ep'}, dimensions={1} | all-to-all | bytes 131072 | tf_op jit(solution)/shard_map/all_to_all | solution.py:88
  20.7 2.3 fusion.20
  23.1 0.7 all-gather.3.cloned.1.call-update
  23.9 0.1 iota_compare_fusion
  23.9 0.1 select_reduce_fusion
  24.0 0.1 copy.42
  24.1 0.1 fusion.70
  24.3 0.1 copy.43
  24.4 0.1 iota_compare_fusion.1
  24.4 29.2 %reduce-scatter.3.cloned.1.call-done = f32[16,1536]{1,0:T(8,128)} async-done(((f32[128,1536]{1,0:T(8,128)}), f32[16,1536]{1,0:T(8,128)}) %reduce-scatter.3.cloned.1.call-update) | async-done | bytes 98320 | tf_op jit(solution)/shard_map/reduce_scatter | solution.py:90
  53.6 0.9 convert.8
  54.6 0.1 multiply_reduce_fusion
  54.7 5.2 %fusion.80 = f32[16,4,1,384]{3,2,1,0:T(1,128)S(1)} fusion(bf16[16,4,128,1]{2,3,1,0:T(2,128)(2,1)S(1)} %reshape.151, bf16[16,4,384,128]{3,2,1,0:T(8,128)(2,1)} %param.30), kind=kOutput, calls=%fused_computation.117 | convolution fusion | flops 6291456 | bytes 6406144 | tf_op jit(solution)/shard_map/shd,shpd->shp/dot_general | solution.py:29
  59.9 0.2 fusion.78
  60.1 0.2 fusion.50
  60.3 0.1 fusion.52
  60.5 1.2 fusion.48
  61.7 0.1 add_convert_fusion
  61.8 22.4 %all-gather.3.cloned.1.call-done = bf16[512,2048]{1,0:T(8,128)(2,1)} async-done(((bf16[512,256]{1,0:T(8,128)(2,1)}), bf16[512,2048]{1,0:T(8,128)(2,1)}) %all-gather.3.cloned.1.call-update) | async-done | bytes 2097168 | tf_op jit(solution)/shard_map/all_gather | solution.py:106
  84.2 2.6 fusion.55
  86.9 41.4 %all-reduce.4.cloned.1.call-done = f32[16,2048]{1,0:T(8,128)} async-done(((f32[16,2048]{1,0:T(8,128)}), f32[16,2048]{1,0:T(8,128)}) %all-reduce.4.cloned.1.call-update) | async-done | bytes 131088 | tf_op jit(solution)/shard_map/psum | solution.py:107
  128.3 1.0 fusion.36
  129.4 0.1 fusion.38
  129.5 10.3 %all_to_all.49 = bf16[16,8,256]{2,0,1:T(8,128)(2,1)S(1)} all-to-all(bf16[16,8,256]{2,0,1:T(8,128)(2,1)S(1)} %bitcast.97), channel_id=1, replica_groups=mesh['ep'=8,'tp'=4] {'ep'}, dimensions={1} | all-to-all | bytes 131072 | tf_op jit(solution)/shard_map/all_to_all | solution.py:111
  139.8 0.9 convolution_convert_fusion.3
  140.8 0.5 all-gather.5.cloned.1.call-update
  141.4 0.1 copy.44
  141.5 0.1 eq.62
  141.7 0.2 select_reduce_fusion.1
  141.9 0.1 reduce_sum.71
  142.0 0.1 copy.45
  142.1 0.3 fusion
  142.4 12.7 %all_to_all.50 = bf16[8,8,2048]{2,1,0:T(8,128)(2,1)S(1)} all-to-all(bf16[8,8,2048]{2,1,0:T(8,128)(2,1)S(1)} %fusion), channel_id=1, replica_groups=mesh['ep'=8,'tp'=4] {'ep'}, dimensions={0} | all-to-all | bytes 524288 | tf_op jit(solution)/shard_map/all_to_all | solution.py:141
  155.1 2.1 fusion.5
  157.2 3.2 %fusion.1 = bf16[8,8,2048]{2,1,0:T(8,128)(2,1)} fusion(bf16[1,512,2048]{2,1,0:T(8,128)(2,1)S(1)} %copy-done, bf16[1,2048,512]{2,1,0:T(8,128)(2,1)} %param.44, bf16[8,8,2048]{2,1,0:T(8,128)(2,1)S(1)} %all_to_all.50, f32[64,512]{1,0:T(8,128)S(1)} %fusion.5), kind=kOutput, calls=%fused_computation.5 | convolution fusion | flops 268763136 | bytes 4849664 | tf_op jit(solution)/shard_map/dot_general | solution.py:147
  160.5 9.1 %reduce-scatter.5.cloned.1.call-done = bf16[16,1024]{1,0:T(8,128)(2,1)} async-done(((bf16[128,1024]{1,0:T(8,128)(2,1)}), bf16[16,1024]{1,0:T(8,128)(2,1)}) %reduce-scatter.5.cloned.1.call-update) | async-done | bytes 32784 | tf_op jit(solution)/shard_map/reduce_scatter | solution.py:113
  169.6 0.8 convert_element_type.119
  170.3 29.4 %all-gather.5.cloned.1.call-done = bf16[512,2048]{1,0:T(8,128)(2,1)} async-done(((bf16[512,256]{1,0:T(8,128)(2,1)}), bf16[512,2048]{1,0:T(8,128)(2,1)}) %all-gather.5.cloned.1.call-update) | async-done | bytes 2097168 | tf_op jit(solution)/shard_map/all_gather | solution.py:122
  199.7 2.6 convolution_convert_fusion.2
  202.4 42.8 %all-reduce.6.cloned.1.call-done = (bf16[16,2048]{1,0:T(8,128)(2,1)}, bf16[8,8,2048]{2,1,0:T(8,128)(2,1)}) async-done(((bf16[16,2048]{1,0:T(8,128)(2,1)}, bf16[8,8,2048]{2,1,0:T(8,128)(2,1)}), (bf16[16,2048]{1,0:T(8,128)(2,1)}, bf16[8,8,2048]{2,1,0:T(8,128)(2,1)})) %all-reduce.6.cloned.1.call-update) | async-done | bytes 327696 | tf_op jit(solution)/shard_map/psum | solution.py:124
  245.2 4.7 %all-to-all-start.2 = ((bf16[8,8,2048]{2,1,0:T(8,128)(2,1)}), bf16[8,8,2048]{2,1,0:T(8,128)(2,1)S(1)}, u32[]{:S(2)}, u32[]{:S(2)}) async-start(bf16[8,8,2048]{2,1,0:T(8,128)(2,1)} %get-tuple-element.6), calls=%async_computation.3 | async-start | bytes 524288 | tf_op jit(solution)/shard_map/all_to_all | solution.py:149
  250.0 0.1 fusion.17
  250.1 9.5 %all-to-all-done.2 = bf16[8,8,2048]{2,1,0:T(8,128)(2,1)S(1)} async-done(((bf16[8,8,2048]{2,1,0:T(8,128)(2,1)}), bf16[8,8,2048]{2,1,0:T(8,128)(2,1)S(1)}, u32[]{:S(2)}, u32[]{:S(2)}) %all-to-all-start.2) | async-done | bytes 262176 | tf_op jit(solution)/shard_map/all_to_all | solution.py:149
  259.7 0.6 gather_fusion
  260.3 0.6 gather_fusion.1
  260.9 0.7 fusion.39
  (62 shorter events, 0.7 us)
Async XLA Ops:
  6.5 150.7 %copy-start = (bf16[1,512,2048]{2,1,0:T(8,128)(2,1)S(1)}, bf16[1,512,2048]{2,1,0:T(8,128)(2,1)}, u32[]{:S(2)}) copy-start(bf16[1,512,2048]{2,1,0:T(8,128)(2,1)} %param.45) | copy-start | bytes 6291460
  6.5 17.3 %copy-start.10 = (s32[16]{0:T(128)S(1)}, s32[16]{0:T(128)}, u32[]{:S(2)}) copy-start(s32[16]{0:T(128)} %param.33) | copy-start | bytes 196
  6.5 17.4 %copy-start.3 = (f32[16,4,384]{2,1,0:T(4,128)S(1)}, f32[16,4,384]{2,1,0:T(4,128)}, u32[]{:S(2)}) copy-start(f32[16,4,384]{2,1,0:T(4,128)} %param.32) | copy-start | bytes 294916
  6.5 17.6 %copy-start.13 = (bf16[2048,4]{0,1:T(4,128)(2,1)S(1)}, bf16[2048,4]{0,1:T(4,128)(2,1)}, u32[]{:S(2)}) copy-start(bf16[2048,4]{0,1:T(4,128)(2,1)} %param.28) | copy-start | bytes 49156
  6.5 17.6 %copy-start.14 = (f32[4]{0:T(128)S(1)}, f32[4]{0:T(128)}, u32[]{:S(2)}) copy-start(f32[4]{0:T(128)} %param.29) | copy-start | bytes 52
  6.5 47.1 %reduce-scatter.3.cloned.1.call-start = ((), (), s32[]{:S(2)}) async-start(), calls=%async_computation.6 | async-start | bytes 884736 | tf_op jit(solution)/shard_map/reduce_scatter | solution.py:90
  23.0 61.2 %all-gather.3.cloned.1.call-start = ((), (), s32[]{:S(2)}) async-start(), calls=%async_computation.7 | async-start | bytes 2359296 | tf_op jit(solution)/shard_map/all_gather | solution.py:106
  23.8 104.6 %all-reduce.4.cloned.1.call-start = ((), (), s32[]{:S(2)}) async-start(), calls=%async_computation.8 | async-start | bytes 262144 | tf_op jit(solution)/shard_map/psum | solution.py:107
  54.7 5.8 %copy-start.1 = (bf16[16,4,384,128]{3,2,1,0:T(8,128)(2,1)S(1)}, bf16[16,4,384,128]{3,2,1,0:T(8,128)(2,1)}, u32[]{:S(2)}) copy-start(bf16[16,4,384,128]{3,2,1,0:T(8,128)(2,1)} %param.31) | copy-start | bytes 18874372
  61.7 66.7 %copy-start.2 = (bf16[16,2048]{1,0:T(8,128)(2,1)S(1)}, bf16[16,2048]{1,0:T(8,128)(2,1)}, u32[]{:S(2)}) copy-start(bf16[16,2048]{1,0:T(8,128)(2,1)} %param.23) | copy-start | bytes 196612
  61.7 67.7 %copy-start.5 = (f32[2048]{0:T(1024)S(1)}, f32[2048]{0:T(1024)}, u32[]{:S(2)}) copy-start(f32[2048]{0:T(1024)} %param.35) | copy-start | bytes 24580
  61.7 78.2 %copy-start.11 = (bf16[256,512]{1,0:T(8,128)(2,1)S(1)}, bf16[256,512]{1,0:T(8,128)(2,1)}, u32[]{:S(2)}) copy-start(bf16[256,512]{1,0:T(8,128)(2,1)} %param.37) | copy-start | bytes 786436
  61.7 78.1 %copy-start.12 = (bf16[256,512]{1,0:T(8,128)(2,1)S(1)}, bf16[256,512]{1,0:T(8,128)(2,1)}, u32[]{:S(2)}) copy-start(bf16[256,512]{1,0:T(8,128)(2,1)} %param.36) | copy-start | bytes 786436
  84.2 57.2 %copy-start.7 = (s32[16,2]{0,1:T(2,128)S(1)}, s32[16,2]{0,1:T(2,128)}, u32[]{:S(2)}) copy-start(s32[16,2]{0,1:T(2,128)} %param.40) | copy-start | bytes 388
  86.9 82.7 %reduce-scatter.5.cloned.1.call-start = ((), (), s32[]{:S(2)}) async-start(), calls=%async_computation.9 | async-start | bytes 294912 | tf_op jit(solution)/shard_map/reduce_scatter | solution.py:113
  140.8 58.9 %all-gather.5.cloned.1.call-start = ((), (), s32[]{:S(2)}) async-start(), calls=%async_computation.10 | async-start | bytes 2359296 | tf_op jit(solution)/shard_map/all_gather | solution.py:122
  141.4 103.8 %all-reduce.6.cloned.1.call-start = ((), (), s32[]{:S(2)}) async-start(), calls=%async_computation.11 | async-start | bytes 655360 | tf_op jit(solution)/shard_map/psum | solution.py:124
  160.4 41.9 %copy-start.8 = (f32[16,2]{0,1:T(2,128)S(1)}, f32[16,2]{0,1:T(2,128)}, u32[]{:S(2)}) copy-start(f32[16,2]{0,1:T(2,128)} %param.42) | copy-start | bytes 388
  160.4 41.9 %copy-start.9 = (f32[16]{0:T(128)S(1)}, f32[16]{0:T(128)}, u32[]{:S(2)}) copy-start(f32[16]{0:T(128)} %param.41) | copy-start | bytes 196
  160.4 89.5 %copy-start.6 = (bf16[2048]{0:T(1024)(128)(2,1)S(1)}, bf16[2048]{0:T(1024)(128)(2,1)}, u32[]{:S(2)}) copy-start(bf16[2048]{0:T(1024)(128)(2,1)} %param.39) | copy-start | bytes 12292
  245.2 15.7 %copy-start.4 = (bf16[16,2048]{1,0:T(8,128)(2,1)S(1)}, bf16[16,2048]{1,0:T(8,128)(2,1)}, u32[]{:S(2)}) copy-start(bf16[16,2048]{1,0:T(8,128)(2,1)} %get-tuple-element.5) | copy-start | bytes 196612
  245.2 14.4 %all-to-all-start.2 = ((bf16[8,8,2048]{2,1,0:T(8,128)(2,1)}), bf16[8,8,2048]{2,1,0:T(8,128)(2,1)S(1)}, u32[]{:S(2)}, u32[]{:S(2)}) async-start(bf16[8,8,2048]{2,1,0:T(8,128)(2,1)} %get-tuple-element.6), calls=%async_computation.3 | async-start | bytes 524288 | tf_op jit(solution)/shard_map/all_to_all | solution.py:149
Sparse Core Ops, SparseCore 0:
  23.2 30.4 reduce-scatter.2
  55.2 28.9 all-gather.2
  87.1 41.2 all-reduce.3
  140.9 28.6 reduce-scatter.4
  171.0 28.6 all-gather.4
  202.5 42.6 all-reduce.5
where the time goes:
time: 269 us; the launch traced here: 268 us
  waiting for transfers between devices  185 us (69%)
  blocking collectives  35.1 us (13%)
  matrix products  20.7 us (8%)
  between operations  13.8 us (5%)
  other arithmetic  6.95 us (3%)
  starting transfers between devices  4.98 us (2%)
    psum x1, waiting for transfers between devices, shards(): lax.psum(dense_terms.astype(jnp.bfloat16), 'tp').astype(jnp.float32)  42.8 us
    psum x1, waiting for transfers between devices, shards(): mixed_heads = lax.psum(head_terms, 'tp')  41.4 us
    all_gather x1, waiting for transfers between devices, shards(): lax.all_gather(dense_down_proj, 'ep', axis=1, tiled=True)  29.4 us
    reduce_scatter x1, waiting for transfers between devices, shards(): lax.psum_scatter(row_term(spread, joined), 'ep', scatter_dimension=0, til...  29.2 us
    all_gather x1, waiting for transfers between devices, shards(): lax.all_gather(output_weight, 'ep', axis=1, tiled=True)  22.4 us
    all_to_all x1, blocking collectives, shards(): lax.all_to_all(outbound, 'ep', split_axis=0, concat_axis=0, tiled=True)  12.7 us
    all_to_all x1, blocking collectives, shards(): lax.all_to_all(normed, 'ep', split_axis=1, concat_axis=0, tiled=True)  12.1 us
    all_to_all x1, blocking collectives, shards(): lax.all_to_all(ffn_in, 'ep', split_axis=1, concat_axis=0, tiled=True)  10.3 us
  transfers between devices with their start and end apart: 7, of which 7 were waited for; matrix products, arithmetic and copies ran while one was open for 6% of the time, Pallas kernels for 0%

commit v1 on v0

v1 whole, which is shorter than its diff:
```python
import functools
import math

import jax
import jax.numpy as jnp
from jax import lax
from jax.experimental import pallas as pl
from jax.experimental.pallas import tpu as pltpu
from jax.sharding import PartitionSpec as P

EPSILON = 1e-06


def rms_scale(values, norm_gain):
    widened = values.astype(jnp.float32)
    return (
        widened
        * lax.rsqrt(jnp.mean(widened * widened, axis=-1, keepdims=True) + EPSILON)
        * norm_gain
    )


def attend(queries, keys_new, values_new, key_cache, value_cache, gate_cache, lengths, log_forget):
    cache_span = key_cache.shape[2]
    score_scale = 1.0 / math.sqrt(key_cache.shape[3])
    positions = jnp.arange(cache_span, dtype=jnp.int32)
    live_mask = positions[None, :] < lengths[:, None]
    last_mask = positions[None, :] == lengths[:, None] - 1
    last_gate = jnp.sum(jnp.where(last_mask[:, None, :], gate_cache, 0.0), axis=-1)
    gate_now = last_gate + log_forget
    scores = (
        jnp.einsum("shd,shpd->shp", queries, key_cache, preferred_element_type=jnp.float32)
        * score_scale
    )
    scores = scores + gate_now[:, :, None] - gate_cache
    scores = jnp.where(live_mask[:, None, :], scores, -jnp.inf)
    own_score = (
        jnp.sum(queries.astype(jnp.float32) * keys_new.astype(jnp.float32), axis=-1) * score_scale
    )
    row_top = jnp.maximum(jnp.max(scores, axis=-1), own_score)
    raised = jnp.exp(scores - row_top[:, :, None])
    own_raised = jnp.exp(own_score - row_top)
    totals = jnp.sum(raised, axis=-1) + own_raised
    weights_low = (raised / totals[:, :, None]).astype(jnp.bfloat16)
    own_prob = (own_raised / totals).astype(jnp.bfloat16)
    attended = jnp.einsum(
        "shp,shpd->shd", weights_low, value_cache, preferred_element_type=jnp.float32
    )
    attended = attended + own_prob.astype(jnp.float32)[:, :, None] * values_new.astype(jnp.float32)
    return attended.astype(jnp.bfloat16)


MESH = pl.DeviceIdType.MESH
F32 = jnp.float32
BF16 = jnp.bfloat16


def fan_out(axis, count, me, source_of, landing, send_sem, recv_sem):
    copies = []
    for step in range(1, count):
        target = lax.rem(me + step, count)
        copy = pltpu.make_async_remote_copy(
            src_ref=source_of(target),
            dst_ref=landing.at[me],
            send_sem=send_sem.at[step],
            recv_sem=recv_sem.at[me],
            device_id={axis: target},
            device_id_type=MESH,
        )
        copy.start()
        copies.append(copy)
    return copies


def collect(axis, count, me, landing, send_sem, recv_sem):
    for step in range(1, count):
        source = lax.rem(me + count - step, count)
        pltpu.make_async_remote_copy(
            src_ref=landing.at[source],
            dst_ref=landing.at[source],
            send_sem=send_sem.at[step],
            recv_sem=recv_sem.at[source],
            device_id={axis: source},
            device_id_type=MESH,
        ).wait_recv()


def spread_rows(axis_ep, axis_tp, n_ep, n_tp, me_ep, me_tp, held, landing, send_sem, recv_sem):
    ratio = n_ep // n_tp
    for part in range(ratio):
        target_ep = me_tp * ratio + part
        for step in range(n_tp):
            target_tp = lax.rem(me_tp + step, n_tp)

            def send():
                pltpu.make_async_remote_copy(
                    src_ref=held.at[part],
                    dst_ref=landing.at[me_ep],
                    send_sem=send_sem.at[part * n_tp + step],
                    recv_sem=recv_sem.at[me_ep],
                    device_id={axis_ep: target_ep, axis_tp: target_tp},
                    device_id_type=MESH,
                ).start()

            if step == 0:
                pl.when(target_ep != me_ep)(send)

                @pl.when(target_ep == me_ep)
                def _():
                    landing[me_ep] = held[part]
            else:
                send()


def spread_wait(axis_ep, axis_tp, n_ep, n_tp, me_ep, me_tp, held, landing, send_sem, recv_sem):
    ratio = n_ep // n_tp
    own_tp = me_ep // ratio
    for step in range(n_ep):
        source = lax.rem(me_ep + n_ep - step, n_ep)

        def arrive():
            pltpu.make_async_remote_copy(
                src_ref=landing.at[source],
                dst_ref=landing.at[source],
                send_sem=send_sem.at[0],
                recv_sem=recv_sem.at[source],
                device_id={axis_ep: source, axis_tp: own_tp},
                device_id_type=MESH,
            ).wait_recv()

        if step == 0:
            pl.when(own_tp != me_tp)(arrive)
        else:
            arrive()


def spread_sent(axis_ep, axis_tp, n_ep, n_tp, me_ep, me_tp, held, landing, send_sem, recv_sem):
    ratio = n_ep // n_tp
    for part in range(ratio):
        target_ep = me_tp * ratio + part
        for step in range(n_tp):
            target_tp = lax.rem(me_tp + step, n_tp)

            def sent():
                pltpu.make_async_remote_copy(
                    src_ref=held.at[part],
                    dst_ref=landing.at[me_ep],
                    send_sem=send_sem.at[part * n_tp + step],
                    recv_sem=recv_sem.at[me_ep],
                    device_id={axis_ep: target_ep, axis_tp: target_tp},
                    device_id_type=MESH,
                ).wait_send()

            if step == 0:
                pl.when(target_ep != me_ep)(sent)
            else:
                sent()


def total_of(ref, count):
    total = ref[0].astype(F32)
    for index in range(1, count):
        total = total + ref[index].astype(F32)
    return total


def dot32(left, right):
    return jnp.dot(left, right, preferred_element_type=F32)


def project_kernel(
    n_ep,
    tokens,
    gain,
    query_weight,
    key_weight,
    value_weight,
    queries,
    keys_new,
    values_new,
    normed_out,
    norm_send,
    norm_land,
    part_send,
    part_land,
    norm_ss,
    norm_rs,
    part_ss,
    part_rs,
):
    me = lax.axis_index("ep")
    barrier = pltpu.get_barrier_semaphore()
    for step in range(1, n_ep):
        pl.semaphore_signal(
            barrier, inc=1, device_id={"ep": lax.rem(me + step, n_ep)}, device_id_type=MESH
        )
    rows, depth = norm_send.shape[1:]
    width = query_weight.shape[1]
    normed = rms_scale(tokens[...], gain[...])
    normed_out[...] = normed.astype(BF16)
    for index in range(n_ep):
        norm_send[index] = normed[:, index * depth : (index + 1) * depth].astype(BF16)
    pl.semaphore_wait(barrier, n_ep - 1)
    sent = fan_out("ep", n_ep, me, lambda t: norm_send.at[t], norm_land, norm_ss, norm_rs)
    norm_land[me] = norm_send[me]
    collect("ep", n_ep, me, norm_land, norm_ss, norm_rs)
    joined = norm_land[...].reshape(n_ep * rows, depth)
    for index, weight in enumerate((query_weight, key_weight, value_weight)):
        part_send[:, :, index * width : (index + 1) * width] = dot32(joined, weight[...]).reshape(
            n_ep, rows, width
        )
    sent += fan_out("ep", n_ep, me, lambda t: part_send.at[t], part_land, part_ss, part_rs)
    part_land[me] = part_send[me]
    collect("ep", n_ep, me, part_land, part_ss, part_rs)
    total = total_of(part_land, n_ep).astype(BF16)
    queries[...] = total[:, :width]
    keys_new[...] = total[:, width : 2 * width]
    values_new[...] = total[:, 2 * width :]
    for copy in sent:
        copy.wait_send()


def project(n_ep, tokens, gain, query_weight, key_weight, value_weight):
    rows, model = tokens.shape
    depth, width = query_weight.shape
    vmem = pl.BlockSpec(memory_space=pltpu.VMEM)
    sems = pltpu.SemaphoreType.DMA((n_ep,))
    head_shape = jax.ShapeDtypeStruct((rows, width), BF16)
    return pl.pallas_call(
        functools.partial(project_kernel, n_ep),
        out_shape=(head_shape,) * 3 + (jax.ShapeDtypeStruct((rows, model), BF16),),
        in_specs=[vmem] * 5,
        out_specs=(vmem,) * 4,
        scratch_shapes=[
            pltpu.VMEM((n_ep, rows, depth), BF16),
            pltpu.VMEM((n_ep, rows, depth), BF16),
            pltpu.VMEM((n_ep, rows, 3 * width), F32),
            pltpu.VMEM((n_ep, rows, 3 * width), F32),
            sems,
            sems,
            sems,
            sems,
        ],
        compiler_params=pltpu.CompilerParams(collective_id=0, has_side_effects=True),
    )(tokens, gain.reshape(1, model), query_weight, key_weight, value_weight)


def feed_kernel(
    n_ep,
    n_tp,
    attended,
    tokens,
    gain,
    output_weight,
    dense_gate,
    dense_up,
    dense_down,
    dense_mix,
    to_slots,
    from_first,
    from_second,
    routes,
    expert_gate,
    expert_up,
    expert_down,
    out,
    gate_held,
    up_held,
    down_held,
    full,
    att_land,
    head_send,
    head_land,
    mix_send,
    mix_land,
    ffn_send,
    ffn_land,
    slot_send,
    slot_land,
    dense_send,
    dense_land,
    expert_send,
    expert_land,
    back_send,
    back_land,
    hidden_send,
    hidden_land,
    down_send,
    down_land,
    tail_send,
    tail_land,
    route_send,
    route_land,
    load_sem,
    att_ss,
    att_rs,
    head_ss,
    head_rs,
    mix_ss,
    mix_rs,
    ffn_ss,
    ffn_rs,
    slot_ss,
    slot_rs,
    dense_ss,
    dense_rs,
    expert_ss,
    expert_rs,
    back_ss,
    back_rs,
    hidden_ss,
    hidden_rs,
    down_ss,
    down_rs,
    tail_ss,
    tail_rs,
    route_ss,
    route_rs,
):
    me = lax.axis_index("ep")
    me_tp = lax.axis_index("tp")
    barrier = pltpu.get_barrier_semaphore()
    everyone = n_ep * n_tp
    place = me * n_tp + me_tp

    def greet(step, carry):
        other = lax.rem(place + step, everyone)
        pl.semaphore_signal(
            barrier,
            inc=1,
            device_id={"ep": other // n_tp, "tp": lax.rem(other, n_tp)},
            device_id_type=MESH,
        )
        return carry

    lax.fori_loop(1, everyone, greet, 0)
    loads = [
        pltpu.make_async_copy(expert_gate, gate_held, load_sem.at[0]),
        pltpu.make_async_copy(expert_up, up_held, load_sem.at[1]),
        pltpu.make_async_copy(expert_down, down_held, load_sem.at[2]),
    ]
    for load in loads:
        load.start()
    pl.semaphore_wait(barrier, everyone - 1)

    rows, model = tokens.shape
    hidden = dense_gate.shape[1]
    depth = dense_gate.shape[0]
    slots = slot_send.shape[1]
    group_rows = n_ep * rows // n_tp
    ratio = n_ep // n_tp
    grid = (n_ep, n_tp, me, me_tp)

    sent = fan_out("ep", n_ep, me, lambda t: attended, att_land, att_ss, att_rs)
    att_land[me] = attended[...]
    collect("ep", n_ep, me, att_land, att_ss, att_rs)
    shares = dot32(att_land[...].reshape(n_ep * rows, hidden), output_weight[...])
    head_send[...] = shares.reshape(n_tp, group_rows, depth)
    sent += fan_out("tp", n_tp, me_tp, lambda t: head_send.at[t], head_land, head_ss, head_rs)
    head_land[me_tp] = head_send[me_tp]
    collect("tp", n_tp, me_tp, head_land, head_ss, head_rs)
    mix_send[...] = total_of(head_land, n_tp).reshape(ratio, rows, depth)
    spread_rows("ep", "tp", *grid, mix_send, mix_land, mix_ss, mix_rs)
    spread_wait("ep", "tp", *grid, mix_send, mix_land, mix_ss, mix_rs)
    for index in range(n_ep):
        full[:, index * depth : (index + 1) * depth] = mix_land[index]
    residual = (tokens[...].astype(F32) + full[...]).astype(BF16)
    ffn_wide = rms_scale(residual, gain[...])
    ffn_in = ffn_wide.astype(BF16)

    for index in range(n_ep):
        ffn_send[index] = ffn_wide[:, index * depth : (index + 1) * depth].astype(BF16)
    sent += fan_out("ep", n_ep, me, lambda t: ffn_send.at[t], ffn_land, ffn_ss, ffn_rs)
    outbound = dot32(to_slots[...], ffn_in)
    for index in range(n_ep):
        slot_send[index] = outbound[index * slots : (index + 1) * slots].astype(BF16)
    sent += fan_out("ep", n_ep, me, lambda t: slot_send.at[t], slot_land, slot_ss, slot_rs)
    ffn_land[me] = ffn_send[me]
    slot_land[me] = slot_send[me]
    mix = jax.nn.sigmoid(
        jnp.sum(ffn_in.astype(F32) * dense_mix[...].astype(F32), axis=-1, keepdims=True)
    )

    collect("ep", n_ep, me, ffn_land, ffn_ss, ffn_rs)
    ffn_rows = ffn_land[...].reshape(n_ep * rows, depth)
    for index, weight in enumerate((dense_gate, dense_up)):
        dense_send[:, :, index * hidden : (index + 1) * hidden] = (
            dot32(ffn_rows, weight[...]).astype(BF16).reshape(n_ep, rows, hidden)
        )
    sent += fan_out("ep", n_ep, me, lambda t: dense_send.at[t], dense_land, dense_ss, dense_rs)
    dense_land[me] = dense_send[me]

    collect("ep", n_ep, me, slot_land, slot_ss, slot_rs)
    for load in loads:
        load.wait()
    slot_rows = jnp.concatenate(
        [slot_land[index].astype(F32) for index in range(n_ep)], axis=0
    ).astype(BF16)
    gate_part = dot32(slot_rows, gate_held[0])
    up_part = dot32(slot_rows, up_held[0])
    expert_hidden = (gate_part / (1.0 + jnp.exp(-gate_part)) * up_part).astype(BF16)
    chunk = model // n_tp
    for index in range(n_tp):
        expert_send[index] = dot32(
            expert_hidden, down_held[0, :, index * chunk : (index + 1) * chunk]
        ).astype(BF16)
    sent += fan_out(
        "tp", n_tp, me_tp, lambda t: expert_send.at[t], expert_land, expert_ss, expert_rs
    )
    expert_land[me_tp] = expert_send[me_tp]

    collect("ep", n_ep, me, dense_land, dense_ss, dense_rs)
    dense_sum = total_of(dense_land, n_ep)
    dense_first = dense_sum[:, :hidden]
    hidden_send[...] = (
        dense_first / (1.0 + jnp.exp(-dense_first)) * dense_sum[:, hidden:]
    ).astype(BF16)
    sent += fan_out("ep", n_ep, me, lambda t: hidden_send, hidden_land, hidden_ss, hidden_rs)
    hidden_land[me] = hidden_send[...]

    collect("tp", n_tp, me_tp, expert_land, expert_ss, expert_rs)
    expert_total = total_of(expert_land, n_tp)
    for index in range(n_ep):
        back_send[index] = expert_total[index * slots : (index + 1) * slots].astype(BF16)
    sent += fan_out("ep", n_ep, me, lambda t: back_send.at[t], back_land, back_ss, back_rs)
    back_land[me] = back_send[me]

    collect("ep", n_ep, me, hidden_land, hidden_ss, hidden_rs)
    down = dot32(hidden_land[...].reshape(n_ep * rows, hidden), dense_down[...])
    down_send[...] = down.astype(BF16).reshape(n_tp, group_rows, depth)
    sent += fan_out("tp", n_tp, me_tp, lambda t: down_send.at[t], down_land, down_ss, down_rs)
    down_land[me_tp] = down_send[me_tp]

    collect("ep", n_ep, me, back_land, back_ss, back_rs)
    back_rows = jnp.concatenate(
        [back_land[index].astype(F32) for index in range(n_ep)], axis=0
    ).astype(BF16)
    route_send[...] = routes[:, 0:1] * dot32(from_first[...], back_rows) + routes[:, 1:2] * dot32(
        from_second[...], back_rows
    )
    sent += fan_out("tp", n_tp, me_tp, lambda t: route_send, route_land, route_ss, route_rs)
    route_land[me_tp] = route_send[...]

    collect("tp", n_tp, me_tp, down_land, down_ss, down_rs)
    tail_send[...] = total_of(down_land, n_tp).astype(BF16).reshape(ratio, rows, depth)
    spread_rows("ep", "tp", *grid, tail_send, tail_land, tail_ss, tail_rs)
    collect("tp", n_tp, me_tp, route_land, route_ss, route_rs)
    spread_wait("ep", "tp", *grid, tail_send, tail_land, tail_ss, tail_rs)
    for index in range(n_ep):
        full[:, index * depth : (index + 1) * depth] = tail_land[index].astype(F32)
    for index in range(n_tp):
        span = slice(index * chunk, (index + 1) * chunk)
        out[:, span] = (
            residual[:, span].astype(F32) + route_land[index] + mix * full[:, span]
        ).astype(BF16)
    for copy in sent:
        copy.wait_send()
    spread_sent("ep", "tp", *grid, mix_send, mix_land, mix_ss, mix_rs)
    spread_sent("ep", "tp", *grid, tail_send, tail_land, tail_ss, tail_rs)


def feed(n_ep, n_tp, slots, attended, tokens, gain, weights, mix, selectors, routes, experts):
    rows, model = tokens.shape
    depth, hidden = weights[1].shape
    group_rows = n_ep * rows // n_tp
    ratio = n_ep // n_tp
    chunk = model // n_tp
    vmem = pl.BlockSpec(memory_space=pltpu.VMEM)
    hbm = pl.BlockSpec(memory_space=pl.ANY)

    def sems(count):
        return [pltpu.SemaphoreType.DMA((count,))] * 2

    def pair(shape, dtype):
        return [pltpu.VMEM(shape, dtype)] * 2

    return pl.pallas_call(
        functools.partial(feed_kernel, n_ep, n_tp),
        out_shape=jax.ShapeDtypeStruct((rows, model), BF16),
        in_specs=[vmem] * 12 + [hbm] * 3,
        out_specs=vmem,
        scratch_shapes=[pltpu.VMEM(item.shape, item.dtype) for item in experts]
        + [pltpu.VMEM((rows, model), F32), pltpu.VMEM((n_ep, rows, hidden), BF16)]
        + pair((n_tp, group_rows, depth), F32)
        + [pltpu.VMEM((ratio, rows, depth), F32), pltpu.VMEM((n_ep, rows, depth), F32)]
        + pair((n_ep, rows, depth), BF16)
        + pair((n_ep, slots, model), BF16)
        + pair((n_ep, rows, 2 * hidden), BF16)
        + pair((n_tp, n_ep * slots, chunk), BF16)
        + pair((n_ep, slots, chunk), BF16)
        + [pltpu.VMEM((rows, hidden), BF16), pltpu.VMEM((n_ep, rows, hidden), BF16)]
        + pair((n_tp, group_rows, depth), BF16)
        + [pltpu.VMEM((ratio, rows, depth), BF16), pltpu.VMEM((n_ep, rows, depth), BF16)]
        + [pltpu.VMEM((rows, chunk), F32), pltpu.VMEM((n_tp, rows, chunk), F32)]
        + [pltpu.SemaphoreType.DMA((3,))]
        + sems(n_ep)
        + sems(n_tp)
        + sems(n_ep)
        + sems(n_ep)
        + sems(n_ep)
        + sems(n_ep)
        + sems(n_tp)
        + sems(n_ep)
        + sems(n_ep)
        + sems(n_tp)
        + sems(n_ep)
        + sems(n_tp),
        compiler_params=pltpu.CompilerParams(
            collective_id=1, has_side_effects=True, vmem_limit_bytes=40 * 1024 * 1024
        ),
    )(attended, tokens, gain.reshape(1, model), *weights, mix.reshape(1, model), *selectors, routes, *experts)


def shards(
    tokens,
    attn_gain,
    query_weight,
    key_weight,
    value_weight,
    forget_weight,
    forget_bias,
    cache_keys,
    cache_values,
    cache_gates,
    lengths,
    output_weight,
    ffn_gain,
    dense_gate_proj,
    dense_up_proj,
    dense_down_proj,
    dense_mix,
    expert_ids,
    group_prob,
    pair_prob,
    expert_gate,
    expert_up,
    expert_down,
):
    seq_count = tokens.shape[0]
    head_count = cache_keys.shape[1]
    head_size = cache_keys.shape[3]
    n_ep = lax.axis_size("ep")
    n_tp = lax.axis_size("tp")
    queries, keys_new, values_new, normed = project(
        n_ep, tokens, attn_gain, query_weight, key_weight, value_weight
    )
    heads = (seq_count, head_count, head_size)
    log_forget = jax.nn.log_sigmoid(
        jnp.dot(normed, forget_weight, preferred_element_type=jnp.float32) + forget_bias
    )
    attended = attend(
        queries.reshape(heads),
        keys_new.reshape(heads),
        values_new.reshape(heads),
        cache_keys,
        cache_values,
        cache_gates,
        lengths,
        log_forget,
    ).reshape(seq_count, head_count * head_size)

    expert_count = n_ep * expert_gate.shape[0]
    capacity = max(4 * seq_count // expert_count, 8)
    slot_total = expert_count * capacity
    picks = expert_ids.reshape(-1)
    same = (picks[:, None] == picks[None, :]).astype(jnp.int32)
    before = jnp.tril(jnp.ones((2 * seq_count, 2 * seq_count), jnp.int32), -1)
    slot_rank = jnp.sum(same * before, axis=1)
    destination = (picks * capacity + slot_rank).reshape(seq_count, 2)
    slot_grid = jnp.arange(slot_total, dtype=jnp.int32)
    select_first = (destination[:, 0:1] == slot_grid[None, :]).astype(jnp.bfloat16)
    select_second = (destination[:, 1:2] == slot_grid[None, :]).astype(jnp.bfloat16)
    to_slots = (select_first + select_second).T
    routes = group_prob[:, None] * pair_prob / jnp.sum(pair_prob, axis=1, keepdims=True)
    return feed(
        n_ep,
        n_tp,
        capacity,
        attended,
        tokens,
        ffn_gain,
        (output_weight, dense_gate_proj, dense_up_proj, dense_down_proj),
        dense_mix,
        (to_slots, select_first, select_second),
        routes,
        (expert_gate, expert_up, expert_down),
    )


def solution(mesh):
    return jax.shard_map(
        shards,
        mesh=mesh,
        in_specs=(
            P("ep", None),
            P(),
            P("ep", "tp"),
            P("ep", "tp"),
            P("ep", "tp"),
            P(None, "tp"),
            P("tp"),
            P("ep", "tp", None, None),
            P("ep", "tp", None, None),
            P("ep", "tp", None),
            P("ep"),
            P("tp", "ep"),
            P(),
            P("ep", "tp"),
            P("ep", "tp"),
            P("tp", "ep"),
            P(),
            P("ep", None),
            P("ep"),
            P("ep", None),
            P("ep", None, "tp"),
            P("ep", None, "tp"),
            P("ep", "tp", None),
        ),
        out_specs=P("ep", None),
        check_vma=False,
    )
```

time: 269 us -> 96 us (0.36)
  waiting for transfers between devices: 185 us -> 0 us
  Pallas kernels: 0 us -> 77.7 us
  blocking collectives: 35.1 us -> 0 us
  between operations: 13.8 us -> 0.33 us
  matrix products: 20.7 us -> 7.35 us
  starting transfers between devices: 4.98 us -> 0 us
  local copies, waits for them, and re-layouts: 1.86 us -> 6.74 us
  other arithmetic: 6.95 us -> 2.88 us
    psum x2 -> x0, waiting for transfers between devices: 84.2 us -> none  [the longest x1 42.8 us: shards(): lax.psum(dense_terms.astype(jnp.bfloat16), 'tp').astype(jnp.float32)]
    pallas_call x0 -> x2, Pallas kernels: none -> 77.7 us  [the longest x1 53.3 us: feed(): pl.pallas_call(functools.partial(feed_kernel, n_ep, n_tp), out_shape=jax....]
    all_gather x2 -> x0, waiting for transfers between devices: 51.8 us -> none  [the longest x1 29.4 us: shards(): lax.all_gather(dense_down_proj, 'ep', axis=1, tiled=True)]
    reduce_scatter x2 -> x0, waiting for transfers between devices: 38.3 us -> none  [the longest x1 29.2 us: shards(): lax.psum_scatter(row_term(spread, joined), 'ep', scatter_dimension=0, til...]
    all_to_all x3 -> x0, blocking collectives: 35.1 us -> none  [the longest x1 12.7 us: shards(): lax.all_to_all(outbound, 'ep', split_axis=0, concat_axis=0, tiled=True)]
    dot_general x8 -> x0, matrix products: 14.2 us -> none  [the longest x2 5.25 us: right_product(): return jnp.dot(left_rows, weight_piece, preferred_element_type=jnp.float32)]
    all_to_all x1 -> x0, waiting for transfers between devices: 9.53 us -> none  [shards(): lax.all_to_all(expert_result.reshape(sources, slots_now, feature).astype(...]
    all_to_all x1 -> x0, starting transfers between devices: 4.74 us -> none  [shards(): lax.all_to_all(expert_result.reshape(sources, slots_now, feature).astype(...]
  transfers between devices with their start and end apart: 7 -> 0, of which waited for: 7 -> 0; matrix products, arithmetic and copies ran while one was open for 6% -> 0% of each run, Pallas kernels for 0% -> 0%
where the time goes in v1:
time: 96 us; the launch traced here: 95 us
  Pallas kernels  77.7 us (81%)
  matrix products  7.35 us (8%)
  local copies, waits for them, and re-layouts  6.74 us (7%)
  other arithmetic  2.88 us (3%)
    pallas_call x1, Pallas kernels, feed(): pl.pallas_call(functools.partial(feed_kernel, n_ep, n_tp), out_shape=jax....  53.3 us
    pallas_call x1, Pallas kernels, project(): pl.pallas_call(functools.partial(project_kernel, n_ep), out_shape=(head_s...  24.4 us
    dot_general x1, matrix products, attend(): jnp.einsum('shd,shpd->shp', queries, key_cache, preferred_element_type=jn...  5.18 us
    unnamed x39, local copies, waits for them, and re-layouts  3.99 us

profile of v1, /device:TPU:0, one launch (start us, length us, event | category | flops | bytes accessed | tf_op | source)
XLA Modules:
  0.0 95.0 jit_solution(11052929584570340587)
XLA Ops:
  0.0 0.0 copy-start
  0.0 24.4 %shard_map.217 = (bf16[16,512]{1,0:T(8,128)(2,1)}, bf16[16,512]{1,0:T(8,128)(2,1)}, bf16[16,512]{1,0:T(8,128)(2,1)}, bf16[16,2048]{1,0:T(8,128)(2,1)}) custom-call(bf16[16,2048]{1,0:T(8,128)(2,1)} %tokens.3, f32[1,2048]{1,0:T(1,128)} %bitcast.32, bf16[256,512]{1,0:T(8,128)(2,1)} %query_weight.1, bf16[256,512]{1,0:T(8,128)(2,1)} %key_weight.1, ...), custom_call_target="tpu_custom_call" | custom-call | tf_op jit(solution)/shard_map/pallas_call | solution.py:229
  24.4 0.7 reshape.94
  25.2 0.7 reshape.90
  25.9 0.1 multiply_reduce_fusion
  26.0 0.7 broadcast_add_fusion
  26.7 0.1 iota_compare_fusion.2
  26.7 1.0 %select_reduce_fusion = f32[16,4]{1,0:T(8,128)S(1)} fusion(f32[16,4,384]{2,1,0:T(4,128)} %param.32, pred[16,384]{1,0:T(8,128)(4,1)S(1)} %iota_compare_fusion.2), kind=kLoop, calls=%fused_computation.9 | loop fusion | flops 49088 | bytes 104704 | tf_op jit(solution)/shard_map/reduce_sum | solution.py:29
  27.7 0.1 copy.50
  27.8 0.0 copy-done
  27.8 1.0 %fusion.16 = f32[16,4]{0,1:T(4,128)S(1)} fusion(f32[16,4]{0,1:T(4,128)S(1)} %copy.50, bf16[16,2048]{1,0:T(8,128)(2,1)} %get-tuple-element.10, bf16[2048,4]{0,1:T(4,128)(2,1)S(1)} %copy-done, f32[4]{0:T(128)} %param.29), kind=kOutput, calls=%fused_computation.37 | convolution fusion | flops 262784 | bytes 82448 | tf_op jit(solution)/shard_map/dot_general | solution.py:549
  28.8 0.1 copy.51
  28.9 0.7 reshape.101
  29.7 0.0 copy-start.10
  29.7 5.2 %fusion.20 = f32[16,4,1,384]{3,2,1,0:T(1,128)S(1)} fusion(bf16[16,4,128,1]{2,3,1,0:T(2,128)(2,1)S(1)} %reshape.101, bf16[16,4,384,128]{3,2,1,0:T(8,128)(2,1)} %param.30), kind=kOutput, calls=%fused_computation.46 | convolution fusion | flops 6291456 | bytes 6406144 | tf_op jit(solution)/shard_map/shd,shpd->shp/dot_general | solution.py:32
  34.8 0.0 copy-done.17
  34.8 0.1 iota_compare_fusion.3
  34.9 0.0 copy-done.11
  34.9 0.0 copy-start.12
  35.0 0.2 fusion.17
  35.2 0.0 copy-start.14
  35.2 0.0 copy-start.15
  35.2 0.0 copy-start.16
  35.2 0.2 fusion.6
  35.4 0.0 copy-start.1
  35.4 0.0 copy-start.4
  35.4 0.0 copy-start.5
  35.4 0.0 copy-start.6
  35.4 0.0 copy-start.7
  35.5 0.0 copy-start.8
  35.5 0.0 copy-start.9
  35.5 0.1 fusion.7
  35.6 1.2 %fusion.4 = f32[16,4,1,128]{3,2,1,0:T(1,128)S(1)} fusion(bf16[16,4,384,128]{3,2,1,0:T(8,128)(2,1)S(1)} %copy-done.10, bf16[16,4,384,1]{2,1,0,3:T(4,128)(2,1)S(1)} %fusion.7), kind=kOutput, calls=%fused_computation.6 | convolution fusion | flops 6291456 | bytes 6373376 | tf_op jit(solution)/shard_map/shp,shpd->shd/dot_general | solution.py:46
  36.9 0.1 add_convert_fusion
  37.0 0.1 copy.52
  37.1 0.1 eq.76
  37.2 0.2 select_reduce_fusion.1
  37.4 0.1 reduce_sum.51
  37.4 0.1 copy.53
  37.6 0.1 fusion.11
  37.6 0.0 copy-done.15
  37.7 0.1 copy.54
  37.8 0.1 broadcast_divide_fusion.routes
  37.9 0.0 copy-start.2
  37.9 1.6 %copy-done.2 = bf16[1,2048,512]{2,1,0:T(8,128)(2,1)S(1)} copy-done((bf16[1,2048,512]{2,1,0:T(8,128)(2,1)S(1)}, bf16[1,2048,512]{2,1,0:T(8,128)(2,1)}, u32[]{:S(2)}) %copy-start.2) | copy-done | bytes 2097176
  39.5 1.6 %copy-done.3 = bf16[1,512,2048]{2,1,0:T(8,128)(2,1)S(1)} copy-done((bf16[1,512,2048]{2,1,0:T(8,128)(2,1)S(1)}, bf16[1,512,2048]{2,1,0:T(8,128)(2,1)}, u32[]{:S(2)}) %copy-start.3) | copy-done | bytes 2097176
  41.1 53.3 %shard_map.218 = bf16[16,2048]{1,0:T(8,128)(2,1)S(1)} custom-call(bf16[16,512]{1,0:T(8,128)(2,1)S(1)} %bitcast.28, bf16[16,2048]{1,0:T(8,128)(2,1)S(1)} %copy-done.4, f32[1,2048]{1,0:T(1,128)S(1)} %bitcast.29, bf16[512,256]{1,0:T(8,128)(2,1)S(1)} %copy-done.5, bf16[256,512]{1,0:T(8,128)(2,1)S(1)} %copy-done.6, bf16[256,512]{1,0:T(8,128)(2,1)S(1)} %copy-done.7, ...), custom_call_target="tpu_custom_call" | custom-call | tf_op jit(solution)/shard_map/pallas_call | solution.py:477
  94.4 0.6 copy.68
  (26 shorter events, 0.2 us)
Async XLA Ops:
  0.0 27.8 %copy-start = (bf16[2048,4]{0,1:T(4,128)(2,1)S(1)}, bf16[2048,4]{0,1:T(4,128)(2,1)}, u32[]{:S(2)}) copy-start(bf16[2048,4]{0,1:T(4,128)(2,1)} %param.28) | copy-start | bytes 49156
  0.0 34.9 %copy-start.11 = (f32[16,4,384]{2,1,0:T(4,128)S(1)}, f32[16,4,384]{2,1,0:T(4,128)}, u32[]{:S(2)}) copy-start(f32[16,4,384]{2,1,0:T(4,128)} %param.32) | copy-start | bytes 294916
  0.0 34.8 %copy-start.17 = (s32[16]{0:T(128)S(1)}, s32[16]{0:T(128)}, u32[]{:S(2)}) copy-start(s32[16]{0:T(128)} %param.33) | copy-start | bytes 196
  29.7 6.0 %copy-start.10 = (bf16[16,4,384,128]{3,2,1,0:T(8,128)(2,1)S(1)}, bf16[16,4,384,128]{3,2,1,0:T(8,128)(2,1)}, u32[]{:S(2)}) copy-start(bf16[16,4,384,128]{3,2,1,0:T(8,128)(2,1)} %param.31) | copy-start | bytes 18874372
  34.9 1.9 %copy-start.12 = (bf16[16,512]{1,0:T(8,128)(2,1)S(1)}, bf16[16,512]{1,0:T(8,128)(2,1)}, u32[]{:S(2)}) copy-start(bf16[16,512]{1,0:T(8,128)(2,1)} %get-tuple-element.12) | copy-start | bytes 49156
  35.1 1.8 %copy-start.13 = (bf16[2048]{0:T(1024)(128)(2,1)S(1)}, bf16[2048]{0:T(1024)(128)(2,1)}, u32[]{:S(2)}) copy-start(bf16[2048]{0:T(1024)(128)(2,1)} %param.39) | copy-start | bytes 12292
  35.2 1.8 %copy-start.14 = (s32[16,2]{0,1:T(2,128)S(1)}, s32[16,2]{0,1:T(2,128)}, u32[]{:S(2)}) copy-start(s32[16,2]{0,1:T(2,128)} %param.40) | copy-start | bytes 388
  35.2 2.5 %copy-start.15 = (f32[16,2]{0,1:T(2,128)S(1)}, f32[16,2]{0,1:T(2,128)}, u32[]{:S(2)}) copy-start(f32[16,2]{0,1:T(2,128)} %param.42) | copy-start | bytes 388
  35.2 2.5 %copy-start.16 = (f32[16]{0:T(128)S(1)}, f32[16]{0:T(128)}, u32[]{:S(2)}) copy-start(f32[16]{0:T(128)} %param.41) | copy-start | bytes 196
  35.4 2.5 %copy-start.1 = (bf16[1,2048,512]{2,1,0:T(8,128)(2,1)S(1)}, bf16[1,2048,512]{2,1,0:T(8,128)(2,1)}, u32[]{:S(2)}) copy-start(bf16[1,2048,512]{2,1,0:T(8,128)(2,1)} %expert_gate.1) | copy-start | bytes 6291460
  35.4 2.4 %copy-start.4 = (bf16[16,2048]{1,0:T(8,128)(2,1)S(1)}, bf16[16,2048]{1,0:T(8,128)(2,1)}, u32[]{:S(2)}) copy-start(bf16[16,2048]{1,0:T(8,128)(2,1)} %tokens.3) | copy-start | bytes 196612
  35.4 2.4 %copy-start.5 = (bf16[512,256]{1,0:T(8,128)(2,1)S(1)}, bf16[512,256]{1,0:T(8,128)(2,1)}, u32[]{:S(2)}) copy-start(bf16[512,256]{1,0:T(8,128)(2,1)} %output_weight.1) | copy-start | bytes 786436
  35.4 2.4 %copy-start.6 = (bf16[256,512]{1,0:T(8,128)(2,1)S(1)}, bf16[256,512]{1,0:T(8,128)(2,1)}, u32[]{:S(2)}) copy-start(bf16[256,512]{1,0:T(8,128)(2,1)} %dense_gate.1) | copy-start | bytes 786436
  35.4 2.4 %copy-start.7 = (bf16[256,512]{1,0:T(8,128)(2,1)S(1)}, bf16[256,512]{1,0:T(8,128)(2,1)}, u32[]{:S(2)}) copy-start(bf16[256,512]{1,0:T(8,128)(2,1)} %dense_up.1) | copy-start | bytes 786436
  35.5 2.4 %copy-start.8 = (bf16[512,256]{1,0:T(8,128)(2,1)S(1)}, bf16[512,256]{1,0:T(8,128)(2,1)}, u32[]{:S(2)}) copy-start(bf16[512,256]{1,0:T(8,128)(2,1)} %dense_down.1) | copy-start | bytes 786436
  35.5 2.4 %copy-start.9 = (f32[2048]{0:T(1024)S(1)}, f32[2048]{0:T(1024)}, u32[]{:S(2)}) copy-start(f32[2048]{0:T(1024)} %param.35) | copy-start | bytes 24580
  37.9 1.6 %copy-start.2 = (bf16[1,2048,512]{2,1,0:T(8,128)(2,1)S(1)}, bf16[1,2048,512]{2,1,0:T(8,128)(2,1)}, u32[]{:S(2)}) copy-start(bf16[1,2048,512]{2,1,0:T(8,128)(2,1)} %expert_up.1) | copy-start | bytes 6291460
  39.5 1.6 %copy-start.3 = (bf16[1,512,2048]{2,1,0:T(8,128)(2,1)S(1)}, bf16[1,512,2048]{2,1,0:T(8,128)(2,1)}, u32[]{:S(2)}) copy-start(bf16[1,512,2048]{2,1,0:T(8,128)(2,1)} %expert_down.1) | copy-start | bytes 6291460

commit v2 on v1

v2 whole, which is shorter than its diff:
```python
import functools
import math

import jax
import jax.numpy as jnp
from jax import lax
from jax.experimental import pallas as pl
from jax.experimental.pallas import tpu as pltpu
from jax.sharding import PartitionSpec as P

EPSILON = 1e-06


def rms_scale(values, norm_gain):
    widened = values.astype(jnp.float32)
    return (
        widened
        * lax.rsqrt(jnp.mean(widened * widened, axis=-1, keepdims=True) + EPSILON)
        * norm_gain
    )


MESH = pl.DeviceIdType.MESH
F32 = jnp.float32
BF16 = jnp.bfloat16


def fan_out(axis, count, me, source_of, landing, send_sem, recv_sem, slot=None):
    copies = []
    place = me if slot is None else slot(me)
    for step in range(1, count):
        target = lax.rem(me + step, count)
        copy = pltpu.make_async_remote_copy(
            src_ref=source_of(target),
            dst_ref=landing.at[place],
            send_sem=send_sem.at[step],
            recv_sem=recv_sem.at[me],
            device_id={axis: target},
            device_id_type=MESH,
        )
        copy.start()
        copies.append(copy)
    return copies


def collect(axis, count, me, landing, send_sem, recv_sem, slot=None):
    for step in range(1, count):
        source = lax.rem(me + count - step, count)
        place = source if slot is None else slot(source)
        pltpu.make_async_remote_copy(
            src_ref=landing.at[place],
            dst_ref=landing.at[place],
            send_sem=send_sem.at[step],
            recv_sem=recv_sem.at[source],
            device_id={axis: source},
            device_id_type=MESH,
        ).wait_recv()


def spread_rows(axis_ep, axis_tp, n_ep, n_tp, me_ep, me_tp, held, landing, send_sem, recv_sem):
    ratio = n_ep // n_tp
    for part in range(ratio):
        target_ep = me_tp * ratio + part
        for step in range(n_tp):
            target_tp = lax.rem(me_tp + step, n_tp)

            def send():
                pltpu.make_async_remote_copy(
                    src_ref=held.at[part],
                    dst_ref=landing.at[me_ep],
                    send_sem=send_sem.at[part * n_tp + step],
                    recv_sem=recv_sem.at[me_ep],
                    device_id={axis_ep: target_ep, axis_tp: target_tp},
                    device_id_type=MESH,
                ).start()

            if step == 0:
                pl.when(target_ep != me_ep)(send)

                @pl.when(target_ep == me_ep)
                def _():
                    landing[me_ep] = held[part]
            else:
                send()


def spread_wait(axis_ep, axis_tp, n_ep, n_tp, me_ep, me_tp, held, landing, send_sem, recv_sem):
    ratio = n_ep // n_tp
    own_tp = me_ep // ratio
    for step in range(n_ep):
        source = lax.rem(me_ep + n_ep - step, n_ep)

        def arrive():
            pltpu.make_async_remote_copy(
                src_ref=landing.at[source],
                dst_ref=landing.at[source],
                send_sem=send_sem.at[0],
                recv_sem=recv_sem.at[source],
                device_id={axis_ep: source, axis_tp: own_tp},
                device_id_type=MESH,
            ).wait_recv()

        if step == 0:
            pl.when(own_tp != me_tp)(arrive)
        else:
            arrive()


def spread_sent(axis_ep, axis_tp, n_ep, n_tp, me_ep, me_tp, held, landing, send_sem, recv_sem):
    ratio = n_ep // n_tp
    for part in range(ratio):
        target_ep = me_tp * ratio + part
        for step in range(n_tp):
            target_tp = lax.rem(me_tp + step, n_tp)

            def sent():
                pltpu.make_async_remote_copy(
                    src_ref=held.at[part],
                    dst_ref=landing.at[me_ep],
                    send_sem=send_sem.at[part * n_tp + step],
                    recv_sem=recv_sem.at[me_ep],
                    device_id={axis_ep: target_ep, axis_tp: target_tp},
                    device_id_type=MESH,
                ).wait_send()

            if step == 0:
                pl.when(target_ep != me_ep)(sent)
            else:
                sent()


def total_of(ref, count):
    total = ref[0].astype(F32)
    for index in range(1, count):
        total = total + ref[index].astype(F32)
    return total


def dot32(left, right):
    return jnp.dot(left, right, preferred_element_type=F32)


def chip_order(index, half):
    return lax.rem(index, 2) * half + index // 2


def pair_copy(axis, me, source, landing, send_sem, recv_sem, slot):
    return pltpu.make_async_remote_copy(
        src_ref=source,
        dst_ref=landing,
        send_sem=send_sem.at[slot],
        recv_sem=recv_sem.at[slot],
        device_id={axis: me + 1 - 2 * lax.rem(me, 2)},
        device_id_type=MESH,
    )


def chip_fan(axis, half, me, held, landing, send_sem, recv_sem):
    chip, core = me // 2, lax.rem(me, 2)
    copies = []
    for step in range(1, half):
        target = lax.rem(chip + step, half)
        copy = pltpu.make_async_remote_copy(
            src_ref=held.at[target],
            dst_ref=landing.at[chip],
            send_sem=send_sem.at[step],
            recv_sem=recv_sem.at[chip],
            device_id={axis: target * 2 + core},
            device_id_type=MESH,
        )
        copy.start()
        copies.append(copy)
    landing[chip] = held[chip]
    return copies


def chip_collect(axis, half, me, landing, send_sem, recv_sem):
    chip, core = me // 2, lax.rem(me, 2)
    for step in range(1, half):
        source = lax.rem(chip + half - step, half)
        pltpu.make_async_remote_copy(
            src_ref=landing.at[source],
            dst_ref=landing.at[source],
            send_sem=send_sem.at[step],
            recv_sem=recv_sem.at[source],
            device_id={axis: source * 2 + core},
            device_id_type=MESH,
        ).wait_recv()


def layer_kernel(
    n_ep,
    n_tp,
    forget_bias,
    tokens,
    attn_gain,
    forget_rows,
    gates,
    lengths,
    gain,
    dense_mix,
    to_slots,
    from_first,
    from_second,
    routes,
    query_weight,
    key_weight,
    value_weight,
    keys,
    values,
    output_weight,
    dense_gate,
    dense_up,
    expert_gate,
    expert_up,
    expert_down,
    dense_down,
    out,
    query_weight_held,
    key_weight_held,
    value_weight_held,
    keys_held,
    values_held,
    output_weight_held,
    dense_gate_held,
    dense_up_held,
    expert_gate_held,
    expert_up_held,
    expert_down_held,
    dense_down_held,
    load_sem,
    norm_send,
    norm_land,
    norm_ss,
    norm_rs,
    part_send,
    part_land,
    part_ss,
    part_rs,
    score_send,
    score_land,
    score_ss,
    score_rs,
    value_send,
    value_land,
    value_ss,
    value_rs,
    query_rows,
    key_rows,
    value_rows,
    forget_logs,
    scores,
    mixed,
    attended,
    full,
    att_land,
    att_ss,
    att_rs,
    head_send,
    head_land,
    head_ss,
    head_rs,
    mix_send,
    mix_land,
    mix_ss,
    mix_rs,
    ffn_send,
    ffn_land,
    ffn_ss,
    ffn_rs,
    slot_send,
    slot_land,
    slot_ss,
    slot_rs,
    pair_send,
    pair_land,
    pair_ss,
    pair_rs,
    dense_send,
    dense_land,
    dense_ss,
    dense_rs,
    expert_send,
    expert_land,
    expert_ss,
    expert_rs,
    back_send,
    back_land,
    back_ss,
    back_rs,
    hidden_send,
    hidden_land,
    hidden_ss,
    hidden_rs,
    down_send,
    down_land,
    down_ss,
    down_rs,
    tail_send,
    tail_land,
    tail_ss,
    tail_rs,
    route_send,
    route_land,
    route_ss,
    route_rs,
):
    me = lax.axis_index("ep")
    me_tp = lax.axis_index("tp")
    barrier = pltpu.get_barrier_semaphore()
    everyone = n_ep * n_tp
    place = me * n_tp + me_tp

    def greet(step, carry):
        other = lax.rem(place + step, everyone)
        pl.semaphore_signal(
            barrier,
            inc=1,
            device_id={"ep": other // n_tp, "tp": lax.rem(other, n_tp)},
            device_id_type=MESH,
        )
        return carry

    lax.fori_loop(1, everyone, greet, 0)
    sources = (query_weight, key_weight, value_weight, keys, values, output_weight, dense_gate, dense_up, expert_gate, expert_up, expert_down, dense_down)
    places = (query_weight_held, key_weight_held, value_weight_held, keys_held, values_held, output_weight_held, dense_gate_held, dense_up_held, expert_gate_held, expert_up_held, expert_down_held, dense_down_held)
    loads = [
        pltpu.make_async_copy(source, place, load_sem.at[index])
        for index, (source, place) in enumerate(zip(sources, places))
    ]
    for load in loads:
        load.start()
    rows, model = tokens.shape
    depth, hidden = query_weight.shape
    heads, span, size = keys.shape[1:]
    slots = slot_send.shape[1]
    group_rows = n_ep * rows // n_tp
    ratio = n_ep // n_tp
    half = n_ep // 2
    chip, core = me // 2, lax.rem(me, 2)
    grid = (n_ep, n_tp, me, me_tp)

    def order(index):
        return chip_order(index, half)

    normed = rms_scale(tokens[...], attn_gain[...])
    for index in range(n_ep):
        norm_send[index] = normed[:, index * depth : (index + 1) * depth].astype(BF16)
    pl.semaphore_wait(barrier, everyone - 1)

    sent = fan_out("ep", n_ep, me, lambda t: norm_send.at[t], norm_land, norm_ss, norm_rs, order)
    norm_land[order(me)] = norm_send[me]
    normed_wide = normed.astype(BF16).astype(F32)
    for head in range(heads):
        logit = forget_bias[0, head] + jnp.sum(
            normed_wide * forget_rows[head : head + 1, :].astype(F32), axis=-1, keepdims=True
        )
        forget_log = jnp.minimum(logit, 0.0) - jnp.log1p(jnp.exp(-jnp.abs(logit)))
        forget_logs[:, head, :] = jnp.broadcast_to(forget_log, (rows, size))
    collect("ep", n_ep, me, norm_land, norm_ss, norm_rs, order)
    joined = norm_land[...].reshape(n_ep * rows, depth)
    for index, weight in enumerate((query_weight_held, key_weight_held, value_weight_held)):
        loads[index].wait()
        part_send[:, :, :, index * hidden : (index + 1) * hidden] = dot32(
            joined, weight[...]
        ).reshape(2, half, rows, hidden)
    swap = pair_copy("ep", me, part_send.at[1 - core], part_land, part_ss, part_rs, 0)
    swap.start()
    swap.wait_recv()
    score_send[...] = part_send[core, :, :, : 2 * hidden] + part_land[:, :, : 2 * hidden]
    sent += chip_fan("ep", half, me, score_send, score_land, score_ss, score_rs)
    value_send[...] = (part_send[core, :, :, 2 * hidden :] + part_land[:, :, 2 * hidden :]).astype(
        BF16
    )
    sent += chip_fan("ep", half, me, value_send, value_land, value_ss, value_rs)
    sent.append(swap)
    chip_collect("ep", half, me, score_land, score_ss, score_rs)
    summed = total_of(score_land, half).astype(BF16).astype(F32)
    for head in range(heads):
        query_rows[:, head, :] = summed[:, head * size : (head + 1) * size]
        key_rows[:, head, :] = summed[:, hidden + head * size : hidden + (head + 1) * size]

    scale = 1.0 / math.sqrt(size)
    loads[3].wait()
    loads[4].wait()

    def score_step(seq, carry):
        for head in range(heads):
            query = query_rows[seq, head : head + 1, :].astype(BF16)
            scores[seq, head : head + 1, :] = lax.dot_general(
                query,
                keys_held[seq, head],
                (((1,), (1,)), ((), ())),
                preferred_element_type=F32,
            )
        return carry

    lax.fori_loop(0, rows, score_step, 0)
    positions = lax.broadcasted_iota(jnp.int32, (rows, heads, span), 2)
    lives = lengths[...]
    gate_all = gates[...]
    last_gate = jnp.sum(jnp.where(positions == lives - 1, gate_all, 0.0), axis=-1, keepdims=True)
    gate_now = last_gate + forget_logs[:, :, 0:1]
    score_all = scores[...] * scale + gate_now - gate_all
    score_all = jnp.where(positions < lives, score_all, -jnp.inf)
    own_score = jnp.sum(query_rows[...] * key_rows[...], axis=-1, keepdims=True) * scale
    row_top = jnp.maximum(jnp.max(score_all, axis=-1, keepdims=True), own_score)
    raised = jnp.exp(score_all - row_top)
    own_raised = jnp.exp(own_score - row_top)
    totals = jnp.sum(raised, axis=-1, keepdims=True) + own_raised
    scores[...] = raised / totals
    own_prob = (own_raised / totals).astype(BF16).astype(F32)

    def value_step(seq, carry):
        for head in range(heads):
            weight = scores[seq, head : head + 1, :].astype(BF16)
            mixed[seq, head : head + 1, :] = dot32(weight, values_held[seq, head])
        return carry

    lax.fori_loop(0, rows, value_step, 0)
    chip_collect("ep", half, me, value_land, value_ss, value_rs)
    value_sum = total_of(value_land, half).astype(BF16).astype(F32)
    for head in range(heads):
        value_rows[:, head, :] = value_sum[:, head * size : (head + 1) * size]
    mixed[...] = mixed[...] + own_prob * value_rows[...]
    for head in range(heads):
        attended[:, head * size : (head + 1) * size] = mixed[:, head, :].astype(BF16)

    sent += fan_out("ep", n_ep, me, lambda t: attended, att_land, att_ss, att_rs)
    att_land[me] = attended[...]
    collect("ep", n_ep, me, att_land, att_ss, att_rs)
    loads[5].wait()
    shares = dot32(att_land[...].reshape(n_ep * rows, hidden), output_weight_held[...])
    head_send[...] = shares.reshape(n_tp, group_rows, depth)
    sent += fan_out("tp", n_tp, me_tp, lambda t: head_send.at[t], head_land, head_ss, head_rs)
    head_land[me_tp] = head_send[me_tp]
    collect("tp", n_tp, me_tp, head_land, head_ss, head_rs)
    mix_send[...] = total_of(head_land, n_tp).reshape(ratio, rows, depth)
    spread_rows("ep", "tp", *grid, mix_send, mix_land, mix_ss, mix_rs)
    spread_wait("ep", "tp", *grid, mix_send, mix_land, mix_ss, mix_rs)
    for index in range(n_ep):
        full[:, index * depth : (index + 1) * depth] = mix_land[index]
    residual = (tokens[...].astype(F32) + full[...]).astype(BF16)
    ffn_wide = rms_scale(residual, gain[...])
    ffn_in = ffn_wide.astype(BF16)

    for index in range(n_ep):
        ffn_send[index] = ffn_wide[:, index * depth : (index + 1) * depth].astype(BF16)
    sent += fan_out("ep", n_ep, me, lambda t: ffn_send.at[t], ffn_land, ffn_ss, ffn_rs, order)
    outbound = dot32(to_slots[...], ffn_in)
    for index in range(n_ep):
        slot_send[index] = outbound[index * slots : (index + 1) * slots].astype(BF16)
    sent += fan_out("ep", n_ep, me, lambda t: slot_send.at[t], slot_land, slot_ss, slot_rs)
    ffn_land[order(me)] = ffn_send[me]
    slot_land[me] = slot_send[me]
    mix = jax.nn.sigmoid(
        jnp.sum(ffn_in.astype(F32) * dense_mix[...].astype(F32), axis=-1, keepdims=True)
    )

    collect("ep", n_ep, me, ffn_land, ffn_ss, ffn_rs, order)
    ffn_rows = ffn_land[...].reshape(n_ep * rows, depth)
    for index, weight in enumerate((dense_gate_held, dense_up_held)):
        loads[6 + index].wait()
        pair_send[:, :, :, index * hidden : (index + 1) * hidden] = dot32(
            ffn_rows, weight[...]
        ).reshape(2, half, rows, hidden)
    swap = pair_copy("ep", me, pair_send.at[1 - core], pair_land, pair_ss, pair_rs, 0)
    swap.start()
    swap.wait_recv()
    sent.append(swap)
    dense_send[...] = (pair_send[core] + pair_land[...]).astype(BF16)
    sent += chip_fan("ep", half, me, dense_send, dense_land, dense_ss, dense_rs)

    collect("ep", n_ep, me, slot_land, slot_ss, slot_rs)
    for load in loads[8:]:
        load.wait()
    slot_rows = jnp.concatenate(
        [slot_land[index].astype(F32) for index in range(n_ep)], axis=0
    ).astype(BF16)
    gate_part = dot32(slot_rows, expert_gate_held[0])
    up_part = dot32(slot_rows, expert_up_held[0])
    expert_hidden = (gate_part / (1.0 + jnp.exp(-gate_part)) * up_part).astype(BF16)
    chunk = model // n_tp
    for index in range(n_tp):
        expert_send[index] = dot32(
            expert_hidden, expert_down_held[0, :, index * chunk : (index + 1) * chunk]
        ).astype(BF16)
    sent += fan_out(
        "tp", n_tp, me_tp, lambda t: expert_send.at[t], expert_land, expert_ss, expert_rs
    )
    expert_land[me_tp] = expert_send[me_tp]

    chip_collect("ep", half, me, dense_land, dense_ss, dense_rs)
    dense_sum = total_of(dense_land, half)
    dense_first = dense_sum[:, :hidden]
    hidden_send[...] = (
        dense_first / (1.0 + jnp.exp(-dense_first)) * dense_sum[:, hidden:]
    ).astype(BF16)
    sent += fan_out("ep", n_ep, me, lambda t: hidden_send, hidden_land, hidden_ss, hidden_rs)
    hidden_land[me] = hidden_send[...]

    collect("tp", n_tp, me_tp, expert_land, expert_ss, expert_rs)
    expert_total = total_of(expert_land, n_tp)
    for index in range(n_ep):
        back_send[index] = expert_total[index * slots : (index + 1) * slots].astype(BF16)
    sent += fan_out("ep", n_ep, me, lambda t: back_send.at[t], back_land, back_ss, back_rs)
    back_land[me] = back_send[me]

    collect("ep", n_ep, me, hidden_land, hidden_ss, hidden_rs)
    down = dot32(hidden_land[...].reshape(n_ep * rows, hidden), dense_down_held[...])
    down_send[...] = down.astype(BF16).reshape(n_tp, group_rows, depth)
    sent += fan_out("tp", n_tp, me_tp, lambda t: down_send.at[t], down_land, down_ss, down_rs)
    down_land[me_tp] = down_send[me_tp]

    collect("ep", n_ep, me, back_land, back_ss, back_rs)
    back_rows = jnp.concatenate(
        [back_land[index].astype(F32) for index in range(n_ep)], axis=0
    ).astype(BF16)
    route_send[...] = routes[:, 0:1] * dot32(from_first[...], back_rows) + routes[:, 1:2] * dot32(
        from_second[...], back_rows
    )
    sent += fan_out("tp", n_tp, me_tp, lambda t: route_send, route_land, route_ss, route_rs)
    route_land[me_tp] = route_send[...]

    collect("tp", n_tp, me_tp, down_land, down_ss, down_rs)
    tail_send[...] = total_of(down_land, n_tp).astype(BF16).reshape(ratio, rows, depth)
    spread_rows("ep", "tp", *grid, tail_send, tail_land, tail_ss, tail_rs)
    collect("tp", n_tp, me_tp, route_land, route_ss, route_rs)
    spread_wait("ep", "tp", *grid, tail_send, tail_land, tail_ss, tail_rs)
    for index in range(n_ep):
        full[:, index * depth : (index + 1) * depth] = tail_land[index].astype(F32)
    for index in range(n_tp):
        span = slice(index * chunk, (index + 1) * chunk)
        out[:, span] = (
            residual[:, span].astype(F32) + route_land[index] + mix * full[:, span]
        ).astype(BF16)
    for copy in sent:
        copy.wait_send()
    spread_sent("ep", "tp", *grid, mix_send, mix_land, mix_ss, mix_rs)
    spread_sent("ep", "tp", *grid, tail_send, tail_land, tail_ss, tail_rs)


def layer(n_ep, n_tp, slots, forget_bias, small, large):
    rows, model = small[0].shape
    depth, hidden = large[0].shape
    heads, span, size = large[3].shape[1:]
    group_rows = n_ep * rows // n_tp
    ratio = n_ep // n_tp
    half = n_ep // 2
    chunk = model // n_tp
    vmem = pl.BlockSpec(memory_space=pltpu.VMEM)
    smem = pl.BlockSpec(memory_space=pltpu.SMEM)
    hbm = pl.BlockSpec(memory_space=pltpu.HBM)
    return pl.pallas_call(
        functools.partial(layer_kernel, n_ep, n_tp),
        out_shape=jax.ShapeDtypeStruct((rows, model), BF16),
        in_specs=[smem] + [vmem] * len(small) + [hbm] * len(large),
        out_specs=vmem,
        scratch_shapes=[
            pltpu.VMEM(large[0].shape, BF16),
            pltpu.VMEM(large[1].shape, BF16),
            pltpu.VMEM(large[2].shape, BF16),
            pltpu.VMEM(large[3].shape, BF16),
            pltpu.VMEM(large[4].shape, BF16),
            pltpu.VMEM(large[5].shape, BF16),
            pltpu.VMEM(large[6].shape, BF16),
            pltpu.VMEM(large[7].shape, BF16),
            pltpu.VMEM(large[8].shape, BF16),
            pltpu.VMEM(large[9].shape, BF16),
            pltpu.VMEM(large[10].shape, BF16),
            pltpu.VMEM(large[11].shape, BF16),
            pltpu.SemaphoreType.DMA((12,)),
            pltpu.VMEM((n_ep, rows, depth), BF16),
            pltpu.VMEM((n_ep, rows, depth), BF16),
            pltpu.SemaphoreType.DMA((n_ep,)),
            pltpu.SemaphoreType.DMA((n_ep,)),
            pltpu.VMEM((2, half, rows, 3 * hidden), F32),
            pltpu.VMEM((half, rows, 3 * hidden), F32),
            pltpu.SemaphoreType.DMA((1,)),
            pltpu.SemaphoreType.DMA((1,)),
            pltpu.VMEM((half, rows, 2 * hidden), F32),
            pltpu.VMEM((half, rows, 2 * hidden), F32),
            pltpu.SemaphoreType.DMA((half,)),
            pltpu.SemaphoreType.DMA((half,)),
            pltpu.VMEM((half, rows, hidden), BF16),
            pltpu.VMEM((half, rows, hidden), BF16),
            pltpu.SemaphoreType.DMA((half,)),
            pltpu.SemaphoreType.DMA((half,)),
            pltpu.VMEM((rows, heads, size), F32),
            pltpu.VMEM((rows, heads, size), F32),
            pltpu.VMEM((rows, heads, size), F32),
            pltpu.VMEM((rows, heads, size), F32),
            pltpu.VMEM((rows, heads, span), F32),
            pltpu.VMEM((rows, heads, size), F32),
            pltpu.VMEM((rows, hidden), BF16),
            pltpu.VMEM((rows, model), F32),
            pltpu.VMEM((n_ep, rows, hidden), BF16),
            pltpu.SemaphoreType.DMA((n_ep,)),
            pltpu.SemaphoreType.DMA((n_ep,)),
            pltpu.VMEM((n_tp, group_rows, depth), F32),
            pltpu.VMEM((n_tp, group_rows, depth), F32),
            pltpu.SemaphoreType.DMA((n_tp,)),
            pltpu.SemaphoreType.DMA((n_tp,)),
            pltpu.VMEM((ratio, rows, depth), F32),
            pltpu.VMEM((n_ep, rows, depth), F32),
            pltpu.SemaphoreType.DMA((n_ep,)),
            pltpu.SemaphoreType.DMA((n_ep,)),
            pltpu.VMEM((n_ep, rows, depth), BF16),
            pltpu.VMEM((n_ep, rows, depth), BF16),
            pltpu.SemaphoreType.DMA((n_ep,)),
            pltpu.SemaphoreType.DMA((n_ep,)),
            pltpu.VMEM((n_ep, slots, model), BF16),
            pltpu.VMEM((n_ep, slots, model), BF16),
            pltpu.SemaphoreType.DMA((n_ep,)),
            pltpu.SemaphoreType.DMA((n_ep,)),
            pltpu.VMEM((2, half, rows, 2 * hidden), F32),
            pltpu.VMEM((half, rows, 2 * hidden), F32),
            pltpu.SemaphoreType.DMA((1,)),
            pltpu.SemaphoreType.DMA((1,)),
            pltpu.VMEM((half, rows, 2 * hidden), BF16),
            pltpu.VMEM((half, rows, 2 * hidden), BF16),
            pltpu.SemaphoreType.DMA((half,)),
            pltpu.SemaphoreType.DMA((half,)),
            pltpu.VMEM((n_tp, n_ep * slots, chunk), BF16),
            pltpu.VMEM((n_tp, n_ep * slots, chunk), BF16),
            pltpu.SemaphoreType.DMA((n_tp,)),
            pltpu.SemaphoreType.DMA((n_tp,)),
            pltpu.VMEM((n_ep, slots, chunk), BF16),
            pltpu.VMEM((n_ep, slots, chunk), BF16),
            pltpu.SemaphoreType.DMA((n_ep,)),
            pltpu.SemaphoreType.DMA((n_ep,)),
            pltpu.VMEM((rows, hidden), BF16),
            pltpu.VMEM((n_ep, rows, hidden), BF16),
            pltpu.SemaphoreType.DMA((n_ep,)),
            pltpu.SemaphoreType.DMA((n_ep,)),
            pltpu.VMEM((n_tp, group_rows, depth), BF16),
            pltpu.VMEM((n_tp, group_rows, depth), BF16),
            pltpu.SemaphoreType.DMA((n_tp,)),
            pltpu.SemaphoreType.DMA((n_tp,)),
            pltpu.VMEM((ratio, rows, depth), BF16),
            pltpu.VMEM((n_ep, rows, depth), BF16),
            pltpu.SemaphoreType.DMA((n_ep,)),
            pltpu.SemaphoreType.DMA((n_ep,)),
            pltpu.VMEM((rows, chunk), F32),
            pltpu.VMEM((n_tp, rows, chunk), F32),
            pltpu.SemaphoreType.DMA((n_tp,)),
            pltpu.SemaphoreType.DMA((n_tp,)),
        ],
        compiler_params=pltpu.CompilerParams(
            collective_id=0, has_side_effects=True, vmem_limit_bytes=60 * 1024 * 1024
        ),
    )(forget_bias, *small, *large)


def shards(
    tokens,
    attn_gain,
    query_weight,
    key_weight,
    value_weight,
    forget_weight,
    forget_bias,
    cache_keys,
    cache_values,
    cache_gates,
    lengths,
    output_weight,
    ffn_gain,
    dense_gate_proj,
    dense_up_proj,
    dense_down_proj,
    dense_mix,
    expert_ids,
    group_prob,
    pair_prob,
    expert_gate,
    expert_up,
    expert_down,
):
    seq_count = tokens.shape[0]
    n_ep = lax.axis_size("ep")
    n_tp = lax.axis_size("tp")
    expert_count = n_ep * expert_gate.shape[0]
    capacity = max(4 * seq_count // expert_count, 8)
    slot_total = expert_count * capacity
    picks = expert_ids.reshape(-1)
    same = (picks[:, None] == picks[None, :]).astype(jnp.int32)
    before = jnp.tril(jnp.ones((2 * seq_count, 2 * seq_count), jnp.int32), -1)
    slot_rank = jnp.sum(same * before, axis=1)
    destination = (picks * capacity + slot_rank).reshape(seq_count, 2)
    slot_grid = jnp.arange(slot_total, dtype=jnp.int32)
    select_first = (destination[:, 0:1] == slot_grid[None, :]).astype(jnp.bfloat16)
    select_second = (destination[:, 1:2] == slot_grid[None, :]).astype(jnp.bfloat16)
    to_slots = (select_first + select_second).T
    routes = group_prob[:, None] * pair_prob / jnp.sum(pair_prob, axis=1, keepdims=True)
    model = (1, tokens.shape[1])
    return layer(
        n_ep,
        n_tp,
        capacity,
        forget_bias.reshape(1, -1),
        (
            tokens,
            attn_gain.reshape(model),
            forget_weight.T,
            cache_gates,
            lengths.reshape(-1, 1, 1),
            ffn_gain.reshape(model),
            dense_mix.reshape(model),
            to_slots,
            select_first,
            select_second,
            routes,
        ),
        (
            query_weight,
            key_weight,
            value_weight,
            cache_keys,
            cache_values,
            output_weight,
            dense_gate_proj,
            dense_up_proj,
            expert_gate,
            expert_up,
            expert_down,
            dense_down_proj,
        ),
    )


def solution(mesh):
    return jax.shard_map(
        shards,
        mesh=mesh,
        in_specs=(
            P("ep", None),
            P(),
            P("ep", "tp"),
            P("ep", "tp"),
            P("ep", "tp"),
            P(None, "tp"),
            P("tp"),
            P("ep", "tp", None, None),
            P("ep", "tp", None, None),
            P("ep", "tp", None),
            P("ep"),
            P("tp", "ep"),
            P(),
            P("ep", "tp"),
            P("ep", "tp"),
            P("tp", "ep"),
            P(),
            P("ep", None),
            P("ep"),
            P("ep", None),
            P("ep", None, "tp"),
            P("ep", None, "tp"),
            P("ep", "tp", None),
        ),
        out_specs=P("ep", None),
        check_vma=False,
    )
```

time: 96 us -> 83.8 us (0.87)
  matrix products: 7.35 us -> 0 us
  Pallas kernels: 77.7 us -> 74.8 us
  local copies, waits for them, and re-layouts: 6.74 us -> 5.19 us
    dot_general x3 -> x0, matrix products: 7.35 us -> none  [the longest x1 5.18 us: attend(): jnp.einsum('shd,shpd->shp', queries, key_cache, preferred_element_type=jn...]
    pallas_call x2 -> x1, Pallas kernels: 77.7 us -> 74.8 us  [layer(): pl.pallas_call(functools.partial(layer_kernel, n_ep, n_tp), out_shape=jax...]
    unnamed x39 -> x2, local copies, waits for them, and re-layouts: 3.99 us -> 2.23 us
    reduce_sum x3 -> x0, other arithmetic: 1.27 us -> none  [the longest x1 1.01 us: attend(): jnp.sum(jnp.where(last_mask[:, None, :], gate_cache, 0.0), axis=-1)]
    reshape x3 -> x2, local copies, waits for them, and re-layouts: 1.48 us -> 2.61 us  [the longest x1 1.32 us: shards(): lengths.reshape(-1, 1, 1)]
where the time goes in v2:
time: 83.8 us; the launch traced here: 83.5 us
  Pallas kernels  74.8 us (89%)
  local copies, waits for them, and re-layouts  5.19 us (6%)
  other arithmetic  3.54 us (4%)
    pallas_call x1, Pallas kernels, layer(): pl.pallas_call(functools.partial(layer_kernel, n_ep, n_tp), out_shape=jax...  74.8 us
    unnamed x2, local copies, waits for them, and re-layouts  2.23 us

profile of v2, /device:TPU:0, one launch (start us, length us, event | category | flops | bytes accessed | tf_op | source)
XLA Modules:
  0.0 83.5 jit_solution(17431382804536141984)
XLA Ops:
  0.0 0.7 fusion.5
  0.7 0.1 copy.44
  0.8 0.7 broadcast_divide_fusion.routes
  1.5 1.3 %copy.46.lengths = s32[16,1,1]{2,1,0:T(1,128)} copy(s32[16,1,1]{0,2,1:T(1,128)} %bitcast.13) | data formatting | bytes 128 | tf_op jit(solution)/shard_map/reshape | solution.py:707
  2.8 1.3 %reshape.26.dense_mix = bf16[1,2048]{1,0:T(2,128)(2,1)} reshape(bf16[2048]{0:T(1024)(128)(2,1)} %param.39) | data formatting | bytes 8192 | tf_op jit(solution)/shard_map/reshape | solution.py:709
  4.1 0.8 copy.42
  4.8 0.1 eq.59
  4.9 0.2 select_reduce_fusion
  5.1 0.1 reduce_sum.21
  5.2 0.1 copy.43
  5.3 0.7 multiply_add_fusion
  6.0 0.7 fusion.3
  6.6 0.6 fusion.2.to_slots
  7.3 74.8 %shard_map.217 = bf16[16,2048]{1,0:T(8,128)(2,1)} custom-call(f32[1,4]{1,0:T(1,128)} %bitcast.12, bf16[16,2048]{1,0:T(8,128)(2,1)} %tokens.1, f32[1,2048]{1,0:T(1,128)} %bitcast.10, bf16[4,2048]{1,0:T(4,128)(2,1)} %bitcast.9, f32[16,4,384]{2,1,0:T(4,128)} %gates.1, s32[16,1,1]{2,1,0:T(1,128)} %copy.46.lengths, f32[1,2048]{1,0:T(1,128)} %bitcast.11, ...), custom_call_target="tpu_custom_call" | custom-call | tf_op jit(solution)/shard_map/pallas_call | solution.py:554
  82.1 1.5 %copy.48 = bf16[16,2048]{1,0:T(8,128)(2,1)} copy(bf16[16,2048]{1,0:T(8,128)(2,1)} %shard_map.217) | data formatting | bytes 131072
  (2 shorter events, 0.0 us)

commit v3 on v2

--- a/solution.py
+++ b/solution.py
@@ -192,12 +192,13 @@
     n_ep,
     n_tp,
     forget_bias,
+    lengths,
     tokens,
     attn_gain,
     forget_rows,
     gates,
-    lengths,
     gain,
+    gain_parts,
     dense_mix,
     to_slots,
     from_first,
@@ -264,10 +265,13 @@
     mix_land,
     mix_ss,
     mix_rs,
-    ffn_send,
-    ffn_land,
-    ffn_ss,
-    ffn_rs,
+    token_send,
+    token_land,
+    token_ss,
+    token_rs,
+    share_land,
+    share_ss,
+    share_rs,
     slot_send,
     slot_land,
     slot_ss,
@@ -346,6 +350,7 @@
     normed = rms_scale(tokens[...], attn_gain[...])
     for index in range(n_ep):
         norm_send[index] = normed[:, index * depth : (index + 1) * depth].astype(BF16)
+        token_send[index] = tokens[:, index * depth : (index + 1) * depth]
     pl.semaphore_wait(barrier, everyone - 1)
 
     sent = fan_out("ep", n_ep, me, lambda t: norm_send.at[t], norm_land, norm_ss, norm_rs, order)
@@ -374,6 +379,8 @@
     )
     sent += chip_fan("ep", half, me, value_send, value_land, value_ss, value_rs)
     sent.append(swap)
+    sent += fan_out("ep", n_ep, me, lambda t: token_send.at[t], token_land, token_ss, token_rs)
+    token_land[me] = token_send[me]
     chip_collect("ep", half, me, score_land, score_ss, score_rs)
     summed = total_of(score_land, half).astype(BF16).astype(F32)
     for head in range(heads):
@@ -395,9 +402,13 @@
             )
         return carry
 
-    lax.fori_loop(0, rows, score_step, 0)
+    lax.fori_loop(0, rows, score_step, 0, unroll=4)
     positions = lax.broadcasted_iota(jnp.int32, (rows, heads, span), 2)
-    lives = lengths[...]
+    sequences = lax.broadcasted_iota(jnp.int32, (rows, heads, size), 0)
+    live_wide = jnp.zeros((rows, heads, size), jnp.int32)
+    for seq in range(rows):
+        live_wide = jnp.where(sequences == seq, lengths[0, seq], live_wide)
+    lives = live_wide[:, :, 0:1]
     gate_all = gates[...]
     last_gate = jnp.sum(jnp.where(positions == lives - 1, gate_all, 0.0), axis=-1, keepdims=True)
     gate_now = last_gate + forget_logs[:, :, 0:1]
@@ -417,7 +428,7 @@
             mixed[seq, head : head + 1, :] = dot32(weight, values_held[seq, head])
         return carry
 
-    lax.fori_loop(0, rows, value_step, 0)
+    lax.fori_loop(0, rows, value_step, 0, unroll=4)
     chip_collect("ep", half, me, value_land, value_ss, value_rs)
     value_sum = total_of(value_land, half).astype(BF16).astype(F32)
     for head in range(heads):
@@ -437,39 +448,56 @@
     collect("tp", n_tp, me_tp, head_land, head_ss, head_rs)
     mix_send[...] = total_of(head_land, n_tp).reshape(ratio, rows, depth)
     spread_rows("ep", "tp", *grid, mix_send, mix_land, mix_ss, mix_rs)
-    spread_wait("ep", "tp", *grid, mix_send, mix_land, mix_ss, mix_rs)
-    for index in range(n_ep):
-        full[:, index * depth : (index + 1) * depth] = mix_land[index]
-    residual = (tokens[...].astype(F32) + full[...]).astype(BF16)
-    ffn_wide = rms_scale(residual, gain[...])
-    ffn_in = ffn_wide.astype(BF16)
-
-    for index in range(n_ep):
-        ffn_send[index] = ffn_wide[:, index * depth : (index + 1) * depth].astype(BF16)
-    sent += fan_out("ep", n_ep, me, lambda t: ffn_send.at[t], ffn_land, ffn_ss, ffn_rs, order)
-    outbound = dot32(to_slots[...], ffn_in)
-    for index in range(n_ep):
-        slot_send[index] = outbound[index * slots : (index + 1) * slots].astype(BF16)
-    sent += fan_out("ep", n_ep, me, lambda t: slot_send.at[t], slot_land, slot_ss, slot_rs)
-    ffn_land[order(me)] = ffn_send[me]
-    slot_land[me] = slot_send[me]
-    mix = jax.nn.sigmoid(
-        jnp.sum(ffn_in.astype(F32) * dense_mix[...].astype(F32), axis=-1, keepdims=True)
-    )
-
-    collect("ep", n_ep, me, ffn_land, ffn_ss, ffn_rs, order)
-    ffn_rows = ffn_land[...].reshape(n_ep * rows, depth)
+    sent += fan_out("tp", n_tp, me_tp, lambda t: mix_send, share_land, share_ss, share_rs)
+    share_land[me_tp] = mix_send[...]
+    collect("ep", n_ep, me, token_land, token_ss, token_rs)
+    collect("tp", n_tp, me_tp, share_land, share_ss, share_rs)
+
+    shared = share_land[...].reshape(n_ep, rows, depth)
+    residual_part = (token_land[...].astype(F32) + shared).astype(BF16)
+    dense_rows = (residual_part.astype(F32) * gain_parts[me]).astype(BF16)
+    dense_rows = dense_rows.reshape(n_ep * rows, depth)
     for index, weight in enumerate((dense_gate_held, dense_up_held)):
         loads[6 + index].wait()
-        pair_send[:, :, :, index * hidden : (index + 1) * hidden] = dot32(
-            ffn_rows, weight[...]
-        ).reshape(2, half, rows, hidden)
+        product = dot32(dense_rows, weight[...])
+        for place in range(n_ep):
+            pair_send[place % 2, place // 2, :, index * hidden : (index + 1) * hidden] = product[
+                place * rows : (place + 1) * rows
+            ]
     swap = pair_copy("ep", me, pair_send.at[1 - core], pair_land, pair_ss, pair_rs, 0)
     swap.start()
     swap.wait_recv()
     sent.append(swap)
     dense_send[...] = (pair_send[core] + pair_land[...]).astype(BF16)
     sent += chip_fan("ep", half, me, dense_send, dense_land, dense_ss, dense_rs)
+
+    spread_wait("ep", "tp", *grid, mix_send, mix_land, mix_ss, mix_rs)
+    for index in range(n_ep):
+        full[:, index * depth : (index + 1) * depth] = mix_land[index]
+    residual = (tokens[...].astype(F32) + full[...]).astype(BF16)
+    residual_wide = residual.astype(F32)
+    row_scale = lax.rsqrt(
+        jnp.mean(residual_wide * residual_wide, axis=-1, keepdims=True) + EPSILON
+    )
+    ffn_in = (residual_wide * row_scale * gain[...]).astype(BF16)
+
+    outbound = dot32(to_slots[...], ffn_in)
+    for index in range(n_ep):
+        slot_send[index] = outbound[index * slots : (index + 1) * slots].astype(BF16)
+    sent += fan_out("ep", n_ep, me, lambda t: slot_send.at[t], slot_land, slot_ss, slot_rs)
+    slot_land[me] = slot_send[me]
+    mix = jax.nn.sigmoid(
+        jnp.sum(ffn_in.astype(F32) * dense_mix[...].astype(F32), axis=-1, keepdims=True)
+    )
+
+    chip_collect("ep", half, me, dense_land, dense_ss, dense_rs)
+    dense_sum = total_of(dense_land, half) * row_scale
+    dense_first = dense_sum[:, :hidden]
+    hidden_send[...] = (
+        dense_first / (1.0 + jnp.exp(-dense_first)) * dense_sum[:, hidden:]
+    ).astype(BF16)
+    sent += fan_out("ep", n_ep, me, lambda t: hidden_send, hidden_land, hidden_ss, hidden_rs)
+    hidden_land[me] = hidden_send[...]
 
     collect("ep", n_ep, me, slot_land, slot_ss, slot_rs)
     for load in loads[8:]:
@@ -490,15 +518,6 @@
     )
     expert_land[me_tp] = expert_send[me_tp]
 
-    chip_collect("ep", half, me, dense_land, dense_ss, dense_rs)
-    dense_sum = total_of(dense_land, half)
-    dense_first = dense_sum[:, :hidden]
-    hidden_send[...] = (
-        dense_first / (1.0 + jnp.exp(-dense_first)) * dense_sum[:, hidden:]
-    ).astype(BF16)
-    sent += fan_out("ep", n_ep, me, lambda t: hidden_send, hidden_land, hidden_ss, hidden_rs)
-    hidden_land[me] = hidden_send[...]
-
     collect("tp", n_tp, me_tp, expert_land, expert_ss, expert_rs)
     expert_total = total_of(expert_land, n_tp)
     for index in range(n_ep):
@@ -540,7 +559,7 @@
     spread_sent("ep", "tp", *grid, tail_send, tail_land, tail_ss, tail_rs)
 
 
-def layer(n_ep, n_tp, slots, forget_bias, small, large):
+def layer(n_ep, n_tp, slots, scalars, small, large):
     rows, model = small[0].shape
     depth, hidden = large[0].shape
     heads, span, size = large[3].shape[1:]
@@ -554,7 +573,7 @@
     return pl.pallas_call(
         functools.partial(layer_kernel, n_ep, n_tp),
         out_shape=jax.ShapeDtypeStruct((rows, model), BF16),
-        in_specs=[smem] + [vmem] * len(small) + [hbm] * len(large),
+        in_specs=[smem] * 2 + [vmem] * len(small) + [hbm] * len(large),
         out_specs=vmem,
         scratch_shapes=[
             pltpu.VMEM(large[0].shape, BF16),
@@ -609,6 +628,9 @@
             pltpu.VMEM((n_ep, rows, depth), BF16),
             pltpu.SemaphoreType.DMA((n_ep,)),
             pltpu.SemaphoreType.DMA((n_ep,)),
+            pltpu.VMEM((n_tp, ratio, rows, depth), F32),
+            pltpu.SemaphoreType.DMA((n_tp,)),
+            pltpu.SemaphoreType.DMA((n_tp,)),
             pltpu.VMEM((n_ep, slots, model), BF16),
             pltpu.VMEM((n_ep, slots, model), BF16),
             pltpu.SemaphoreType.DMA((n_ep,)),
@@ -649,7 +671,7 @@
         compiler_params=pltpu.CompilerParams(
             collective_id=0, has_side_effects=True, vmem_limit_bytes=60 * 1024 * 1024
         ),
-    )(forget_bias, *small, *large)
+    )(*scalars, *small, *large)
 
 
 def shards(
@@ -698,14 +720,14 @@
         n_ep,
         n_tp,
         capacity,
-        forget_bias.reshape(1, -1),
+        (forget_bias.reshape(1, -1), lengths.reshape(1, -1)),
         (
             tokens,
             attn_gain.reshape(model),
             forget_weight.T,
             cache_gates,
-            lengths.reshape(-1, 1, 1),
             ffn_gain.reshape(model),
+            ffn_gain.reshape(n_ep, 1, -1),
             dense_mix.reshape(model),
             to_slots,
             select_first,

time: 83.8 us -> 79.6 us (0.950)
  Pallas kernels: 74.8 us -> 71.9 us
  local copies, waits for them, and re-layouts: 5.19 us -> 3.86 us
    pallas_call x1, Pallas kernels: 74.8 us -> 71.9 us  [layer(): pl.pallas_call(functools.partial(layer_kernel, n_ep, n_tp), out_shape=jax...]
    reshape x1 -> x0, local copies, waits for them, and re-layouts: 1.32 us -> none  [shards(): lengths.reshape(-1, 1, 1)]
where the time goes in v3:
time: 79.6 us; the launch traced here: 79.3 us
  Pallas kernels  71.9 us (90%)
  local copies, waits for them, and re-layouts  3.86 us (5%)
  other arithmetic  3.54 us (4%)
    pallas_call x1, Pallas kernels, layer(): pl.pallas_call(functools.partial(layer_kernel, n_ep, n_tp), out_shape=jax...  71.9 us
    unnamed x2, local copies, waits for them, and re-layouts  2.23 us

profile of v3, /device:TPU:0, one launch (start us, length us, event | category | flops | bytes accessed | tf_op | source)
XLA Modules:
  0.0 79.3 jit_solution(41530277424294660)
XLA Ops:
  0.0 0.7 fusion.5
  0.7 0.1 copy.41
  0.8 0.7 broadcast_divide_fusion.routes
  1.5 1.3 %reshape.30.dense_mix = bf16[1,2048]{1,0:T(2,128)(2,1)} reshape(bf16[2048]{0:T(1024)(128)(2,1)} %param.39) | data formatting | bytes 8192 | tf_op jit(solution)/shard_map/reshape | solution.py:731
  2.7 0.8 copy.39
  3.5 0.1 eq.59
  3.6 0.2 select_reduce_fusion
  3.8 0.1 reduce_sum.21
  3.9 0.1 copy.40
  3.9 0.7 multiply_add_fusion
  4.7 0.7 fusion.3
  5.3 0.6 fusion.2.to_slots
  5.9 71.9 %shard_map.217 = bf16[16,2048]{1,0:T(8,128)(2,1)} custom-call(f32[1,4]{1,0:T(1,128)} %bitcast.14, s32[1,16]{1,0:T(1,128)} %bitcast.15, bf16[16,2048]{1,0:T(8,128)(2,1)} %tokens.1, f32[1,2048]{1,0:T(1,128)} %bitcast.13, bf16[4,2048]{1,0:T(4,128)(2,1)} %bitcast.12, f32[16,4,384]{2,1,0:T(4,128)} %gates.1, f32[1,2048]{1,0:T(1,128)} %bitcast.10, ...), custom_call_target="tpu_custom_call" | custom-call | tf_op jit(solution)/shard_map/pallas_call | solution.py:573
  77.8 1.5 %copy.44 = bf16[16,2048]{1,0:T(8,128)(2,1)} copy(bf16[16,2048]{1,0:T(8,128)(2,1)} %shard_map.217) | data formatting | bytes 131072
  (2 shorter events, 0.0 us)
